TPU v7x, 256 devices: a whole 4x4x8 slice. The times are simulated.
256 devices in a mesh: ep: 64 (over z, y, core), tp: 4 (over x).
Axes of the slice: x: 4, y: 4, z: 8, core: 2. Of those that a mesh axis runs over, the one named last changes fastest.
Arguments:
- queries: bfloat16 [12288, 2048], P('ep', 'tp'), may hold values from -5 to 5
- keys: bfloat16 [12288, 512], P('ep', 'tp'), may hold values from -5 to 5
- values: bfloat16 [12288, 512], P('ep', 'tp'), may hold values from -6 to 6
- query_gain: float32 [128], replicated, may hold values from 0.6 to 6
- key_gain: float32 [128], replicated, may hold values from 0.6 to 6
- out_weight: bfloat16 [2048, 2048], P('tp'), may hold values from -0.125 to 0.125
- mixer_gain: float32 [2048], replicated, may hold values from 0.1 to 1.9
- expert_in: bfloat16 [32768, 2048], P(('ep', 'tp')), may hold values from -6 to 6
- routes: int32 [32768, 2], P(('ep', 'tp')), may hold values from 0 to 63, all different within a row; in each aligned block of 128 rows (0 to 127, 128 to 255, ...) at most 6 rows name the same one
- route_weights: float32 [32768, 2], P(('ep', 'tp')), may hold values from 0.2 to 1
- expert_gain: float32 [2048], replicated, may hold values from 0.5 to 4
- gate_w: bfloat16 [64, 2048, 2048], P('ep', None, 'tp'), may hold values from -0.125 to 0.125
- up_w: bfloat16 [64, 2048, 2048], P('ep', None, 'tp'), may hold values from -0.125 to 0.125
- down_w: bfloat16 [64, 2048, 2048], P('ep', 'tp'), may hold values from -0.125 to 0.125
- ffn_out_gain: float32 [2048], replicated, may hold values from 0.1 to 1.9
Outputs:
- mixer_out: bfloat16 [12288, 2048], P(('ep', 'tp'))
- expert_out: bfloat16 [32768, 2048], P(('ep', 'tp'))
Inputs may be any that keep to these rules, and one draw needn't show every extreme that they name: `routes`: each row names 2 different experts. Among the rows of one device no expert is named by more than 6 rows, and in every draw some expert is named by exactly 6 rows of some device.
All inputs are finite; a program needn't handle non-finite values.
Results may differ from a plain program's by a relative error of at most 0.015.
The roundings to bfloat16 on the way count: a program that leaves them out, or rounds other values in their place, can miss the bound.
Values may be sent and summed in bfloat16 or wider, within the bound.
A program may use at most 128 MiB of HBM per device.

v0:
```python
import jax
import jax.numpy as jnp
from jax import lax
from jax.sharding import Mesh
from jax.sharding import PartitionSpec as P

HEAD = 128
GRID_W = 64
EP = ("ep_0", "ep_1", "ep_2")
EP_TP = ("ep_0", "ep_1", "ep_2", "tp")


norm_eps = 1e-06
rope_base = 10000.0
clamp_limit = 7.0
sigmoid_slope = 1.702


def whole_of(array, axes, dim):
    if not axes:
        return array
    nearer = lax.all_gather(array, axes[-1], axis=dim, tiled=True)
    return whole_of(nearer, axes[:-1], dim)


def in_blocks(array, dim, peers):
    before, after = (array.shape[:dim], array.shape[dim + 1 :])
    return jnp.moveaxis(array.reshape(*before, peers, -1, *after), dim, 0)


def summed_on_arrival(array, axis, dim):
    blocks = in_blocks(array, dim, lax.axis_size(axis))
    arrived = lax.all_to_all(blocks, axis, split_axis=0, concat_axis=0, tiled=True)
    return arrived.astype(jnp.float32).sum(axis=0)


def rms_scale(values_in, gain):
    return (
        values_in
        * lax.rsqrt(jnp.mean(values_in * values_in, axis=-1, keepdims=True) + norm_eps)
        * gain
    )


def turn_pair(halfpart, cosine, sine):
    first_part, second_part = jnp.split(halfpart, 2, axis=-1)
    return jnp.concatenate(
        [first_part * cosine - second_part * sine, second_part * cosine + first_part * sine],
        axis=-1,
    )


def grid_rotate(field, position):
    half_width = field.shape[-1] // 2
    inverse = rope_base ** (-jnp.arange(0, half_width, 2, dtype=jnp.float32) / half_width)
    grid_row = (position // GRID_W).astype(jnp.float32)
    grid_col = (position % GRID_W).astype(jnp.float32)
    row_angle = (grid_row[:, None] * inverse[None, :])[:, None, :]
    col_angle = (grid_col[:, None] * inverse[None, :])[:, None, :]
    return jnp.concatenate(
        [
            turn_pair(field[..., :half_width], jnp.cos(row_angle), jnp.sin(row_angle)),
            turn_pair(field[..., half_width:], jnp.cos(col_angle), jnp.sin(col_angle)),
        ],
        axis=-1,
    )


def clamped_unit(gate_pre, up_pre):
    gate_cut = jnp.minimum(gate_pre, clamp_limit)
    up_cut = jnp.clip(up_pre, -clamp_limit, clamp_limit)
    return ((up_cut + 1.0) * gate_cut * jax.nn.sigmoid(sigmoid_slope * gate_cut)).astype(
        jnp.bfloat16
    )


def mixer_half(queries, keys, values, query_gain, key_gain, out_weight, mixer_gain):
    local_rows = queries.shape[0]
    kv_local = keys.shape[1] // HEAD
    group_size = queries.shape[1] // HEAD // kv_local
    position = lax.axis_index(EP) * local_rows + jnp.arange(local_rows, dtype=jnp.int32)
    query_f = queries.astype(jnp.float32).reshape(local_rows, kv_local * group_size, HEAD)
    query_norm = grid_rotate(rms_scale(query_f, query_gain), position).astype(jnp.bfloat16)
    query_norm = query_norm.reshape(local_rows, kv_local, group_size, HEAD)
    key_f = keys.astype(jnp.float32).reshape(local_rows, kv_local, HEAD)
    key_norm = grid_rotate(rms_scale(key_f, key_gain), position).astype(jnp.bfloat16)
    key_norm = key_norm.reshape(local_rows, kv_local * HEAD)
    score_scale = HEAD ** (-0.5)
    initial = (
        jnp.full((kv_local, group_size, local_rows), -1e30, jnp.float32),
        jnp.zeros((kv_local, group_size, local_rows), jnp.float32),
        jnp.zeros((kv_local, group_size, local_rows, HEAD), jnp.float32),
    )
    key_piece = whole_of(key_norm, ("ep_2", "ep_0", "ep_1"), 0)
    value_piece = whole_of(values, ("ep_2", "ep_0", "ep_1"), 0)
    piece_rows = key_piece.shape[0]
    block_rows = 1
    for candidate in range(min(piece_rows, 1024), 0, -1):
        if piece_rows % candidate == 0:
            block_rows = candidate
            break
    key_blocks = key_piece.reshape(piece_rows // block_rows, block_rows, kv_local, HEAD)
    value_blocks = value_piece.reshape(piece_rows // block_rows, block_rows, kv_local, HEAD)

    def one_block(state, blocks_in):
        running_max, running_total, weighted = state
        key_block, value_block = blocks_in
        scores = (
            jnp.einsum("qhgd,khd->hgqk", query_norm, key_block, preferred_element_type=jnp.float32)
            * score_scale
        )
        new_max = jnp.maximum(running_max, jnp.max(scores, axis=-1))
        factor = jnp.exp(running_max - new_max)
        expo = jnp.exp(scores - new_max[..., None])
        new_total = running_total * factor + jnp.sum(expo, axis=-1)
        new_weighted = weighted * factor[..., None] + jnp.einsum(
            "hgqk,khd->hgqd",
            expo.astype(jnp.bfloat16),
            value_block,
            preferred_element_type=jnp.float32,
        )
        return ((new_max, new_total, new_weighted), None)

    state_out, unused = lax.scan(one_block, initial, (key_blocks, value_blocks))
    final_max, final_total, weighted = state_out
    attended = (weighted / final_total[..., None]).astype(jnp.bfloat16)
    attended = jnp.transpose(attended, (2, 0, 1, 3)).reshape(
        local_rows, kv_local * group_size * HEAD
    )
    share_rows = local_rows // lax.axis_size("tp")
    selected = lax.slice_in_dim(attended, 0, share_rows * lax.axis_size("tp"), axis=0)
    projected = summed_on_arrival(
        jnp.dot(selected, out_weight, preferred_element_type=jnp.float32).astype(jnp.bfloat16),
        "tp",
        0,
    )
    return rms_scale(projected, mixer_gain).astype(jnp.bfloat16)


def expert_half(expert_in, routes, route_weights, expert_gain, gate_w, up_w, down_w, ffn_out_gain):
    tok_rows = expert_in.shape[0]
    model_width = expert_in.shape[1]
    top_count = routes.shape[1]
    expert_count = lax.axis_size(EP)
    capacity = max(2, (3 * tok_rows * top_count + 2 * expert_count - 1) // (2 * expert_count))
    normed = rms_scale(expert_in.astype(jnp.float32), expert_gain).astype(jnp.bfloat16)
    pair_expert = routes.reshape(-1)
    pair_count = pair_expert.shape[0]
    one_hot = (pair_expert[:, None] == jnp.arange(expert_count, dtype=jnp.int32)[None, :]).astype(
        jnp.int32
    )
    pair_rank = jnp.sum(jnp.cumsum(one_hot, axis=0) * one_hot, axis=1) - 1
    pair_slot = pair_expert * capacity + pair_rank
    slot_pair = (
        jnp.full((expert_count * capacity,), pair_count, jnp.int32)
        .at[pair_slot]
        .set(jnp.arange(pair_count, dtype=jnp.int32))
    )
    padded = jnp.concatenate([normed, jnp.zeros((1, model_width), jnp.bfloat16)], axis=0)
    outgoing = padded[slot_pair // top_count].reshape(expert_count, capacity, model_width)
    gate_local = gate_w[0]
    up_local = up_w[0]
    down_local = down_w[0]
    arrived = lax.all_to_all(outgoing, EP, split_axis=0, concat_axis=0, tiled=True)
    flat_rows = arrived.reshape(-1, model_width)
    shard_rows = lax.all_gather(flat_rows, "tp", axis=0, tiled=True)
    hidden = clamped_unit(
        jnp.dot(shard_rows, gate_local, preferred_element_type=jnp.float32),
        jnp.dot(shard_rows, up_local, preferred_element_type=jnp.float32),
    )
    selected = lax.slice_in_dim(hidden, 0, flat_rows.shape[0] * lax.axis_size("tp"), axis=0)
    result = summed_on_arrival(
        jnp.dot(selected, down_local, preferred_element_type=jnp.float32).astype(jnp.bfloat16),
        "tp",
        0,
    )
    finished = result.astype(jnp.bfloat16).reshape(arrived.shape)
    returned = lax.all_to_all(finished, EP, split_axis=0, concat_axis=0, tiled=True)
    pair_result = returned.reshape(-1, model_width)[pair_slot].reshape(
        tok_rows, top_count, model_width
    )
    combined = jnp.einsum("tk,tkd->td", route_weights, pair_result.astype(jnp.float32))
    return rms_scale(combined, ffn_out_gain).astype(jnp.bfloat16)


def local(
    queries,
    keys,
    values,
    query_gain,
    key_gain,
    out_weight,
    mixer_gain,
    expert_in,
    routes,
    route_weights,
    expert_gain,
    gate_w,
    up_w,
    down_w,
    ffn_out_gain,
):
    mixer_out = mixer_half(queries, keys, values, query_gain, key_gain, out_weight, mixer_gain)
    expert_out = expert_half(
        expert_in, routes, route_weights, expert_gain, gate_w, up_w, down_w, ffn_out_gain
    )
    return (mixer_out, expert_out)


def solution(mesh):
    split = Mesh(mesh.devices.reshape(8, 4, 2, mesh.shape["tp"]), ("ep_0", "ep_1", "ep_2", "tp"))
    return jax.shard_map(
        local,
        mesh=split,
        in_specs=(
            P(EP, "tp"),
            P(EP, "tp"),
            P(EP, "tp"),
            P(),
            P(),
            P("tp", None),
            P(),
            P(EP_TP, None),
            P(EP_TP, None),
            P(EP_TP, None),
            P(),
            P(EP, None, "tp"),
            P(EP, None, "tp"),
            P(EP, "tp", None),
            P(),
        ),
        out_specs=(P(EP_TP, None), P(EP_TP, None)),
        check_vma=False,
    )
```

profile of v0, /device:TPU:1, one launch (start us, length us, event | category | flops | bytes accessed | tf_op | source)
XLA Modules:
  0.0 383.9 jit_solution(1543116212559423939)
XLA Ops:
  10.2 11.7 %all_gather.21 = bf16[768,128]{1,0:T(8,128)(2,1)} all-gather(bf16[192,128]{1,0:T(8,128)(2,1)S(1)} %pad_maximum_fusion.1), channel_id=1, replica_groups=mesh['ep_0'=8,'ep_1'=4,'ep_2'=2,'tp'=4] {'ep_1'}, dimensions={0}, use_global_device_ids=true | all-gather | bytes 245760 | tf_op jit(solution)/shard_map/all_gather | solution.py:22
  28.8 3.1 gather_fusion
  32.0 3.7 reshape.500
  35.7 14.4 %all-to-all-start.1 = ((bf16[64,6,2048]{2,1,0:T(8,128)(2,1)}), bf16[64,6,2048]{2,1,0:T(8,128)(2,1)}, u32[]{:S(2)}, u32[]{:S(2)}) async-start(bf16[64,6,2048]{2,1,0:T(8,128)(2,1)} %reshape.500), calls=%async_computation.1 | async-start | bytes 4194304 | tf_op jit(solution)/shard_map/all_to_all | solution.py:164
  50.1 12.7 %all_gather.24 = bf16[768,128]{1,0:T(8,128)(2,1)} all-gather(bf16[192,128]{1,0:T(8,128)(2,1)S(1)} %copy-done.3), channel_id=1, replica_groups=mesh['ep_0'=8,'ep_1'=4,'ep_2'=2,'tp'=4] {'ep_1'}, dimensions={0}, use_global_device_ids=true | all-gather | bytes 245760 | tf_op jit(solution)/shard_map/all_gather | solution.py:22
  62.9 47.5 %all-to-all-done.1 = bf16[64,6,2048]{2,1,0:T(8,128)(2,1)} async-done(((bf16[64,6,2048]{2,1,0:T(8,128)(2,1)}), bf16[64,6,2048]{2,1,0:T(8,128)(2,1)}, u32[]{:S(2)}, u32[]{:S(2)}) %all-to-all-start.1) | async-done | bytes 1572896 | tf_op jit(solution)/shard_map/all_to_all | solution.py:164
  110.4 3.7 reshape.501
  116.8 7.9 %all-gather.10.cloned.1.call-done = bf16[6144,128]{1,0:T(8,128)(2,1)} async-done(((bf16[768,128]{1,0:T(8,128)(2,1)}), bf16[6144,128]{1,0:T(8,128)(2,1)}) %all-gather.10.cloned.1.call-update) | async-done | bytes 1572880 | tf_op jit(solution)/shard_map/all_gather | solution.py:22
  125.1 1.7 fusion.41
  128.1 66.8 %all-gather.14.cloned.1.call-done = bf16[1536,2048]{1,0:T(8,128)(2,1)} async-done(((bf16[384,2048]{1,0:T(8,128)(2,1)}), bf16[1536,2048]{1,0:T(8,128)(2,1)}) %all-gather.14.cloned.1.call-update) | async-done | bytes 6291472 | tf_op jit(solution)/shard_map/all_gather | solution.py:166
  195.0 8.5 %convolution_minimum_fusion = f32[1536,512]{1,0:T(8,128)} fusion(bf16[1536,2048]{1,0:T(8,128)(2,1)} %all-gather.14.cloned.1.call-done, bf16[1,2048,512]{2,1,0:T(8,128)(2,1)} %param.28), kind=kOutput, calls=%fused_computation.31 | convolution fusion | flops 3222011904 | bytes 11534336 | tf_op jit(solution)/shard_map/dot_general | solution.py:168
  203.5 11.9 %convolution_convert_fusion = bf16[1536,2048]{1,0:T(8,128)(2,1)} fusion(bf16[1,512,2048]{2,1,0:T(8,128)(2,1)S(1)} %copy-done, f32[1536,512]{1,0:T(8,128)} %convolution_minimum_fusion, bf16[1536,2048]{1,0:T(8,128)(2,1)} %all-gather.14.cloned.1.call-done, bf16[1,2048,512]{2,1,0:T(8,128)(2,1)} %param.29), kind=kOutput, calls=%fused_computation.29 | convolution fusion | flops 6452674560 | bytes 19922944 | tf_op jit(solution)/shard_map/dot_general | solution.py:173
  215.5 5.2 %all-to-all-start.2 = ((bf16[4,384,2048]{2,1,0:T(8,128)(2,1)}), bf16[4,384,2048]{2,1,0:T(8,128)(2,1)}, u32[]{:S(2)}, u32[]{:S(2)}) async-start(bf16[4,384,2048]{2,1,0:T(8,128)(2,1)} %bitcast.150), calls=%async_computation.2 | async-start | bytes 12582912 | tf_op jit(solution)/shard_map/all_to_all | solution.py:33
  220.7 15.4 %all-gather.12.cloned.1.call-done = bf16[12288,128]{1,0:T(8,128)(2,1)} async-done(((bf16[6144,128]{1,0:T(8,128)(2,1)}), bf16[12288,128]{1,0:T(8,128)(2,1)}) %all-gather.12.cloned.1.call-update) | async-done | bytes 3145744 | tf_op jit(solution)/shard_map/all_gather | solution.py:22
  236.1 49.7 %while.15 = (s32[]{:T(128)}, f32[1,4,192]{2,1,0:T(4,128)S(1)}, f32[1,4,192]{2,1,0:T(4,128)S(1)}, f32[1,4,192,128]{3,2,1,0:T(8,128)S(1)}, bf16[12,1024,1,128]{3,1...) while((s32[]{:T(128)}, f32[1,4,192]{2,1,0:T(4,128)S(1)}, ...), condition=%wide.region_5.6_spmd.clone, body=%wide.region_2.5_spmd.clone.sunk | while | flops 409244160 | bytes 10994793 | solution.py:124
  242.0 1.7 fusion.98
  246.1 1.7 fusion.98
  250.3 1.7 fusion.98
  254.4 1.7 fusion.98
  258.6 1.7 fusion.98
  262.7 1.7 fusion.98
  279.3 1.7 fusion.98
  283.4 1.7 fusion.98
  286.2 3.1 convolution_convert_fusion.1
  289.3 2.0 all-to-all-done.2
  291.3 3.7 all-to-all-start
  295.0 4.2 %reduce_sum.92 = bf16[384,2048]{1,0:T(8,128)(2,1)S(1)} reduce(bf16[4,384,2048]{2,1,0:T(8,128)(2,1)} %all-to-all-done.2, bf16[]{:T(256)} %constant.128.clone.1), dimensions={0}, to_apply=%region_13.14 | reduce | flops 2359296 | bytes 7864322 | tf_op jit(solution)/shard_map/reduce_sum | solution.py:34
  300.9 4.3 %all-to-all-done = bf16[4,48,2048]{2,1,0:T(8,128)(2,1)S(1)} async-done(((bf16[4,48,2048]{2,1,0:T(8,128)(2,1)}), bf16[4,48,2048]{2,1,0:T(8,128)(2,1)S(1)}, u32[]{:S(2)}, u32[]{:S(2)}) %all-to-all-start) | async-done | bytes 786464 | tf_op jit(solution)/shard_map/all_to_all | solution.py:33
  305.1 13.1 %all-to-all-start.3 = ((bf16[64,6,2048]{2,1,0:T(8,128)(2,1)}), bf16[64,6,2048]{2,1,0:T(8,128)(2,1)}, u32[]{:S(2)}, u32[]{:S(2)}) async-start(bf16[64,6,2048]{2,1,0:T(8,128)(2,1)} %reshape.503), calls=%async_computation.3 | async-start | bytes 4194304 | tf_op jit(solution)/shard_map/all_to_all | solution.py:178
  319.5 48.4 %all-to-all-done.3 = bf16[64,6,2048]{2,1,0:T(8,128)(2,1)} async-done(((bf16[64,6,2048]{2,1,0:T(8,128)(2,1)}), bf16[64,6,2048]{2,1,0:T(8,128)(2,1)}, u32[]{:S(2)}, u32[]{:S(2)}) %all-to-all-start.3) | async-done | bytes 1572896 | tf_op jit(solution)/shard_map/all_to_all | solution.py:178
  367.8 2.6 reshape.504
  373.3 2.5 fusion.83
  (145 shorter events, 57.5 us)
Async XLA Ops:
  7.2 196.4 %copy-start = (bf16[1,512,2048]{2,1,0:T(8,128)(2,1)S(1)}, bf16[1,512,2048]{2,1,0:T(8,128)(2,1)}, u32[]{:S(2)}) copy-start(bf16[1,512,2048]{2,1,0:T(8,128)(2,1)} %param.30) | copy-start | bytes 6291460
  7.2 107.0 %all-gather.6.cloned.1.call-start = ((), (), s32[]{:S(2)}) async-start(), calls=%async_computation.4 | async-start | bytes 1769472 | tf_op jit(solution)/shard_map/all_gather | solution.py:22
  32.0 18.2 %copy-start.3 = (bf16[192,128]{1,0:T(8,128)(2,1)S(1)}, bf16[192,128]{1,0:T(8,128)(2,1)}, u32[]{:S(2)}) copy-start(bf16[192,128]{1,0:T(8,128)(2,1)} %param.19) | copy-start | bytes 147460
  35.7 74.7 %all-to-all-start.1 = ((bf16[64,6,2048]{2,1,0:T(8,128)(2,1)}), bf16[64,6,2048]{2,1,0:T(8,128)(2,1)}, u32[]{:S(2)}, u32[]{:S(2)}) async-start(bf16[64,6,2048]{2,1,0:T(8,128)(2,1)} %reshape.500), calls=%async_computation.1 | async-start | bytes 4194304 | tf_op jit(solution)/shard_map/all_to_all | solution.py:164
  50.1 74.7 %all-gather.10.cloned.1.call-start = ((), (), s32[]{:S(2)}) async-start(), calls=%async_computation.6 | async-start | bytes 1769472 | tf_op jit(solution)/shard_map/all_gather | solution.py:22
  62.8 52.1 %copy-start.2 = (bf16[192,512]{1,0:T(8,128)(2,1)S(1)}, bf16[192,512]{1,0:T(8,128)(2,1)}, u32[]{:S(2)}) copy-start(bf16[192,512]{1,0:T(8,128)(2,1)} %param.17) | copy-start | bytes 589828
  62.8 132.2 %all-gather.14.cloned.1.call-start = ((), (), s32[]{:S(2)}) async-start(), calls=%async_computation.8 | async-start | bytes 7864320 | tf_op jit(solution)/shard_map/all_gather | solution.py:166
  114.1 10.7 %copy-start.7 = (f32[128]{0:T(128)S(1)}, f32[128]{0:T(128)}, u32[]{:S(2)}) copy-start(f32[128]{0:T(128)} %param.20) | copy-start | bytes 1540
  114.1 106.6 %all-gather.8.cloned.1.call-start = ((), (), s32[]{:S(2)}) async-start(), calls=%async_computation.5 | async-start | bytes 4718592 | tf_op jit(solution)/shard_map/all_gather | solution.py:22
  114.7 121.4 %all-gather.12.cloned.1.call-start = ((), (), s32[]{:S(2)}) async-start(), calls=%async_computation.7 | async-start | bytes 4718592 | tf_op jit(solution)/shard_map/all_gather | solution.py:22
  215.5 75.8 %all-to-all-start.2 = ((bf16[4,384,2048]{2,1,0:T(8,128)(2,1)}), bf16[4,384,2048]{2,1,0:T(8,128)(2,1)}, u32[]{:S(2)}, u32[]{:S(2)}) async-start(bf16[4,384,2048]{2,1,0:T(8,128)(2,1)} %bitcast.150), calls=%async_computation.2 | async-start | bytes 12582912 | tf_op jit(solution)/shard_map/all_to_all | solution.py:33
  291.3 13.9 %all-to-all-start = ((bf16[4,48,2048]{2,1,0:T(8,128)(2,1)}), bf16[4,48,2048]{2,1,0:T(8,128)(2,1)S(1)}, u32[]{:S(2)}, u32[]{:S(2)}) async-start(bf16[4,48,2048]{2,1,0:T(8,128)(2,1)} %bitcast.13), calls=%async_computation | async-start | bytes 1572864 | tf_op jit(solution)/shard_map/all_to_all | solution.py:33
  299.2 19.0 %copy-start.6 = (f32[128,2]{0,1:T(2,128)S(1)}, f32[128,2]{0,1:T(2,128)}, u32[]{:S(2)}) copy-start(f32[128,2]{0,1:T(2,128)} %param.26) | copy-start | bytes 3076
  300.9 17.8 %copy-start.4 = (f32[2048]{0:T(1024)S(1)}, f32[2048]{0:T(1024)}, u32[]{:S(2)}) copy-start(f32[2048]{0:T(1024)} %param.23) | copy-start | bytes 24580
  305.1 62.7 %all-to-all-start.3 = ((bf16[64,6,2048]{2,1,0:T(8,128)(2,1)}), bf16[64,6,2048]{2,1,0:T(8,128)(2,1)}, u32[]{:S(2)}, u32[]{:S(2)}) async-start(bf16[64,6,2048]{2,1,0:T(8,128)(2,1)} %reshape.503), calls=%async_computation.3 | async-start | bytes 4194304 | tf_op jit(solution)/shard_map/all_to_all | solution.py:178
  371.8 5.6 %copy-start.1 = (bf16[1,512,2048]{2,1,0:T(8,128)(2,1)S(1)}, bf16[1,512,2048]{2,1,0:T(8,128)(2,1)}, u32[]{:S(2)}) copy-start(bf16[1,512,2048]{2,1,0:T(8,128)(2,1)} %param.30) | copy-start | bytes 6291460
  373.3 2.9 copy-start.5
Sparse Core Ops, SparseCore 0:
  22.0 52.0 all-gather.5
  75.9 48.8 all-gather.9
  126.6 68.3 all-gather.13
  196.6 19.0 all-gather.7
  217.4 18.7 all-gather.11
where the time goes:
time: 386 us; the launch traced here: 384 us
  waiting for transfers between devices  193 us (50%)
  matrix products  66.5 us (17%)
  starting transfers between devices  36.8 us (10%)
  other arithmetic  26.9 us (7%)
  blocking collectives  24.3 us (6%)
  local copies, waits for them, and re-layouts  21.8 us (6%)
  between operations  14.2 us (4%)
    all_gather x1, waiting for transfers between devices, expert_half(): shard_rows = lax.all_gather(flat_rows, 'tp', axis=0, tiled=True)  66.8 us
    all_to_all x1, waiting for transfers between devices, expert_half(): lax.all_to_all(finished, EP, split_axis=0, concat_axis=0, tiled=True)  48.4 us
    all_to_all x1, waiting for transfers between devices, expert_half(): lax.all_to_all(outgoing, EP, split_axis=0, concat_axis=0, tiled=True)  47.5 us
    all_gather x2, blocking collectives, whole_of(): nearer = lax.all_gather(array, axes[-1], axis=dim, tiled=True)  24.3 us
    all_gather x4, waiting for transfers between devices, whole_of(): nearer = lax.all_gather(array, axes[-1], axis=dim, tiled=True)  23.4 us
    dot_general x12, matrix products, one_block(): jnp.einsum('hgqk,khd->hgqd', expo.astype(jnp.bfloat16), value_block, pref...  20.3 us
    dot_general x12, matrix products, one_block(): jnp.einsum('qhgd,khd->hgqk', query_norm, key_block, preferred_element_typ...  20.1 us
    all_to_all x1, starting transfers between devices, expert_half(): lax.all_to_all(outgoing, EP, split_axis=0, concat_axis=0, tiled=True)  14.4 us
  transfers between devices with their start and end apart: 9, of which 7 were waited for; matrix products, arithmetic and copies ran while one was open for 27% of the time, Pallas kernels for 0%

commit v1 on v0

--- a/solution.py
+++ b/solution.py
@@ -1,6 +1,11 @@
+import functools
+
 import jax
 import jax.numpy as jnp
+import numpy as np
 from jax import lax
+from jax.experimental import pallas as pl
+from jax.experimental.pallas import tpu as pltpu
 from jax.sharding import Mesh
 from jax.sharding import PartitionSpec as P
 
@@ -8,12 +13,19 @@
 GRID_W = 64
 EP = ("ep_0", "ep_1", "ep_2")
 EP_TP = ("ep_0", "ep_1", "ep_2", "tp")
-
+MESH = pl.DeviceIdType.MESH
+BF = jnp.bfloat16
+F32 = jnp.float32
 
 norm_eps = 1e-06
 rope_base = 10000.0
 clamp_limit = 7.0
 sigmoid_slope = 1.702
+
+PL = 8
+CAP = 6
+SUB = 8
+ROWS = PL * CAP
 
 
 def whole_of(array, axes, dim):
@@ -63,14 +75,6 @@
             turn_pair(field[..., half_width:], jnp.cos(col_angle), jnp.sin(col_angle)),
         ],
         axis=-1,
-    )
-
-
-def clamped_unit(gate_pre, up_pre):
-    gate_cut = jnp.minimum(gate_pre, clamp_limit)
-    up_cut = jnp.clip(up_pre, -clamp_limit, clamp_limit)
-    return ((up_cut + 1.0) * gate_cut * jax.nn.sigmoid(sigmoid_slope * gate_cut)).astype(
-        jnp.bfloat16
     )
 
 
@@ -94,11 +98,7 @@
     key_piece = whole_of(key_norm, ("ep_2", "ep_0", "ep_1"), 0)
     value_piece = whole_of(values, ("ep_2", "ep_0", "ep_1"), 0)
     piece_rows = key_piece.shape[0]
-    block_rows = 1
-    for candidate in range(min(piece_rows, 1024), 0, -1):
-        if piece_rows % candidate == 0:
-            block_rows = candidate
-            break
+    block_rows = 1024
     key_blocks = key_piece.reshape(piece_rows // block_rows, block_rows, kv_local, HEAD)
     value_blocks = value_piece.reshape(piece_rows // block_rows, block_rows, kv_local, HEAD)
 
@@ -127,60 +127,442 @@
     attended = jnp.transpose(attended, (2, 0, 1, 3)).reshape(
         local_rows, kv_local * group_size * HEAD
     )
-    share_rows = local_rows // lax.axis_size("tp")
-    selected = lax.slice_in_dim(attended, 0, share_rows * lax.axis_size("tp"), axis=0)
     projected = summed_on_arrival(
-        jnp.dot(selected, out_weight, preferred_element_type=jnp.float32).astype(jnp.bfloat16),
+        jnp.dot(attended, out_weight, preferred_element_type=jnp.float32).astype(jnp.bfloat16),
         "tp",
         0,
     )
     return rms_scale(projected, mixer_gain).astype(jnp.bfloat16)
 
 
+def dot(a, b):
+    return jnp.dot(a, b, preferred_element_type=F32)
+
+
+def one_hot(cond):
+    return jnp.where(cond, 1.0, 0.0).astype(BF)
+
+
+def experts_kernel(
+    nz,
+    x_ref,
+    routes_ref,
+    routes_t_ref,
+    rw_ref,
+    eg_ref,
+    fg_ref,
+    pin_ref,
+    pout_ref,
+    gate_hbm,
+    up_hbm,
+    down_hbm,
+    out_ref,
+    normed,
+    outgoing,
+    arr,
+    xall,
+    part,
+    rs1,
+    rs2,
+    ret_out,
+    ret_in,
+    ret_rows,
+    wgu,
+    wd,
+    combined,
+    w_sem,
+    d_send,
+    d_recv,
+    ag_send,
+    ag_recv,
+    rs_send,
+    rs1_recv,
+    rs2_recv,
+    r_send,
+    r_recv,
+):
+    z = lax.axis_index("ep_0")
+    p_me = lax.axis_index("ep_1") * 2 + lax.axis_index("ep_2")
+    x_me = lax.axis_index("tp")
+    right = {"tp": lax.rem(x_me + 1, 4)}
+    left = {"tp": lax.rem(x_me + 3, 4)}
+    tok, width = x_ref.shape
+    half = width // 2
+    sub_w = width // SUB
+    ff = wd.shape[0]
+    n_exp = nz * PL
+
+    def peer(zz, p):
+        return {"ep_0": zz, "ep_1": p // 2, "ep_2": lax.rem(p, 2)}
+
+    def away(i):
+        return jnp.where(lax.rem(i, 2) == 1, (i + 1) // 2, -(i // 2))
+
+    def plane(i):
+        return lax.rem(z + away(i) + nz, nz)
+
+    def mirror(i):
+        other = jnp.where(lax.rem(i, 2) == 1, i + 1, i - 1)
+        return jnp.where((i == 0) | (i == nz - 1), i, other)
+
+    barrier = pltpu.get_barrier_semaphore()
+
+    @pl.loop(1, n_exp)
+    def _(j):
+        to = lax.rem(z * PL + p_me + j, n_exp)
+        pl.semaphore_signal(
+            barrier, inc=1, device_id=peer(to // PL, lax.rem(to, PL)), device_id_type=MESH
+        )
+
+    pl.semaphore_signal(barrier, inc=1, device_id=left, device_id_type=MESH)
+    pl.semaphore_signal(barrier, inc=1, device_id=right, device_id_type=MESH)
+
+    w_copies = [
+        pltpu.make_async_copy(gate_hbm.at[0], wgu.at[:, pl.ds(0, ff)], w_sem.at[0]),
+        pltpu.make_async_copy(up_hbm.at[0], wgu.at[:, pl.ds(ff, ff)], w_sem.at[1]),
+        pltpu.make_async_copy(down_hbm.at[0], wd, w_sem.at[2]),
+    ]
+    for copy in w_copies:
+        copy.start()
+
+    xf = x_ref[...].astype(F32)
+    normed[...] = rms_scale(xf, eg_ref[...]).astype(BF)
+
+    def base_of(e):
+        o = (lax.shift_right_logical(e, 3) - z + nz) & (nz - 1)
+        idx = jnp.where(o == 0, 0, jnp.where(o <= nz // 2, 2 * o - 1, 2 * (nz - o)))
+        return idx * ROWS + (e & 7) * CAP
+
+    e_rows = lax.broadcasted_iota(jnp.int32, (n_exp, tok), 0)
+    t_a = lax.broadcasted_iota(jnp.int32, (tok, tok), 0)
+    t_b = lax.broadcasted_iota(jnp.int32, (tok, tok), 1)
+    before_t = one_hot(t_a < t_b)
+    before = one_hot(t_b < t_a)
+    oh0 = e_rows == routes_t_ref[0:1, :]
+    oh1 = e_rows == routes_t_ref[1:2, :]
+    rank0 = dot(one_hot(oh0), before_t)
+    rank1 = dot(one_hot(oh1), before_t) + jnp.sum(
+        jnp.where(oh0, 1.0, 0.0), axis=1, keepdims=True
+    )
+    base = base_of(e_rows).astype(F32)
+    place0 = jnp.sum(jnp.where(oh0, base + rank0, 0.0), axis=0, keepdims=True).astype(jnp.int32)
+    place1 = jnp.sum(jnp.where(oh1, base + rank1, 0.0), axis=0, keepdims=True).astype(jnp.int32)
+    slots = lax.broadcasted_iota(jnp.int32, (nz * ROWS, tok), 0)
+    pick = one_hot((slots == place0) | (slots == place1))
+
+    pl.semaphore_wait(barrier, n_exp - 1 + 2)
+
+    def stack_pieces(rows):
+        return jnp.concatenate(
+            [rows[:, q * sub_w : (q + 1) * sub_w] for q in range(SUB)], axis=0
+        )
+
+    def join_pieces(stacked):
+        return jnp.concatenate(
+            [stacked[q * ROWS : (q + 1) * ROWS, :] for q in range(SUB)], axis=1
+        )
+
+    def to_blocks(rows):
+        blocks = dot(pout_ref[...], stack_pieces(rows)).astype(BF)
+        return blocks.reshape(PL, ROWS, sub_w)
+
+    def to_rows(blocks):
+        flat = blocks.reshape(PL * ROWS, sub_w)
+        return join_pieces(dot(pin_ref[...], flat).astype(BF))
+
+    def dispatch(i, p):
+        return pltpu.make_async_remote_copy(
+            src_ref=outgoing.at[i, p],
+            dst_ref=arr.at[mirror(i), p_me],
+            send_sem=d_send.at[i],
+            recv_sem=d_recv.at[mirror(i)],
+            device_id=peer(plane(i), p),
+            device_id_type=MESH,
+        )
+
+    def give_back(i, p):
+        return pltpu.make_async_remote_copy(
+            src_ref=ret_out.at[i, p],
+            dst_ref=ret_in.at[mirror(i), p_me],
+            send_sem=r_send.at[i],
+            recv_sem=r_recv.at[mirror(i)],
+            device_id=peer(plane(i), p),
+            device_id_type=MESH,
+        )
+
+    def to_plane(i, make):
+        @pl.when(i == 0)
+        def _():
+            @pl.loop(1, PL)
+            def _(j):
+                make(i, lax.rem(p_me + j, PL)).start()
+
+        @pl.when(i > 0)
+        def _():
+            @pl.loop(0, PL)
+            def _(j):
+                make(i, lax.rem(p_me + j, PL)).start()
+
+    def wait_bytes(ref, sem):
+        pltpu.make_async_copy(ref, ref, sem).wait()
+
+    def wait_plane(i, ref, sem):
+        @pl.when(i == 0)
+        def _():
+            wait_bytes(ref.at[0, pl.ds(0, PL - 1)], sem.at[0])
+
+        @pl.when(i > 0)
+        def _():
+            wait_bytes(ref.at[i], sem.at[i])
+
+    for i in range(nz):
+        rows = dot(pick[i * ROWS : (i + 1) * ROWS, :], normed[...]).astype(BF)
+        outgoing[i] = to_blocks(rows)
+        if i == 0:
+            arr[0, p_me] = outgoing[0, p_me]
+        to_plane(jnp.int32(i), dispatch)
+
+    def x_copy(src, dst, send, recv, to):
+        return pltpu.make_async_remote_copy(
+            src_ref=src, dst_ref=dst, send_sem=send, recv_sem=recv, device_id=to,
+            device_id_type=MESH,
+        )
+
+    cols_a, cols_b = pl.ds(0, half), pl.ds(half, half)
+
+    def ag_right(k):
+        return x_copy(xall.at[k, 0], xall.at[k, 1], ag_send.at[k, 0], ag_recv.at[k, 0], right)
+
+    def ag_left(k):
+        return x_copy(xall.at[k, 0], xall.at[k, 2], ag_send.at[k, 1], ag_recv.at[k, 1], left)
+
+    def fwd_right(k):
+        return x_copy(
+            xall.at[k, 1, :, cols_a], xall.at[k, 3, :, cols_a],
+            ag_send.at[k, 2], ag_recv.at[k, 2], right,
+        )
+
+    def fwd_left(k):
+        return x_copy(
+            xall.at[k, 2, :, cols_b], xall.at[k, 3, :, cols_b],
+            ag_send.at[k, 3], ag_recv.at[k, 3], left,
+        )
+
+    def rs_far_left(k):
+        return x_copy(
+            part.at[k, 3, :, cols_a], rs1.at[k, 0], rs_send.at[k, 0], rs1_recv.at[k, 0], left
+        )
+
+    def rs_far_right(k):
+        return x_copy(
+            part.at[k, 3, :, cols_b], rs1.at[k, 1], rs_send.at[k, 1], rs1_recv.at[k, 1], right
+        )
+
+    def rs_near_left(k, c, s):
+        return x_copy(
+            part.at[k, 1, :, c], rs2.at[k, 1, :, c], rs_send.at[k, s], rs2_recv.at[k, s - 2], left
+        )
+
+    def rs_near_right(k, c, s):
+        return x_copy(
+            part.at[k, 2, :, c], rs2.at[k, 0, :, c], rs_send.at[k, s], rs2_recv.at[k, s - 2], right
+        )
+
+    def rs_copies(k):
+        return (
+            rs_far_left(k),
+            rs_far_right(k),
+            rs_near_left(k, cols_a, 2),
+            rs_near_left(k, cols_b, 3),
+            rs_near_right(k, cols_a, 4),
+            rs_near_right(k, cols_b, 5),
+        )
+
+    @pl.loop(0, nz + 5)
+    def _(step):
+        @pl.when(step < nz)
+        def _():
+            k = step
+            wait_plane(k, arr, d_recv)
+            xall[k, 0] = to_rows(arr[k])
+            ag_right(k).start()
+            ag_left(k).start()
+
+        @pl.when((step >= 1) & (step < nz + 1))
+        def _():
+            k = step - 1
+            ag_right(k).wait_recv()
+            fwd_right(k).start()
+            ag_left(k).wait_recv()
+            fwd_left(k).start()
+
+        @pl.when((step >= 2) & (step < nz + 2))
+        def _():
+            k = step - 2
+            fwd_right(k).wait_recv()
+            fwd_left(k).wait_recv()
+
+            @pl.when(step == 2)
+            def _():
+                for copy in w_copies:
+                    copy.wait()
+
+            rows = xall[k].reshape(4 * ROWS, width)
+            pre = dot(rows, wgu[...])
+            gate_cut = jnp.minimum(pre[:, :ff], clamp_limit)
+            up_cut = jnp.clip(pre[:, ff:], -clamp_limit, clamp_limit)
+            hidden = (
+                (up_cut + 1.0) * gate_cut * (1.0 / (1.0 + jnp.exp(-sigmoid_slope * gate_cut)))
+            ).astype(BF)
+            part[k] = dot(hidden, wd[...]).astype(BF).reshape(4, ROWS, width)
+            rs_far_left(k).start()
+            rs_far_right(k).start()
+            rs_near_left(k, cols_b, 3).start()
+            rs_near_right(k, cols_a, 4).start()
+
+        @pl.when((step >= 3) & (step < nz + 3))
+        def _():
+            k = step - 3
+            rs_far_left(k).wait_recv()
+            part[k, 1, :, cols_a] = (
+                part[k, 1, :, cols_a].astype(F32) + rs1[k, 0].astype(F32)
+            ).astype(BF)
+            rs_near_left(k, cols_a, 2).start()
+            rs_far_right(k).wait_recv()
+            part[k, 2, :, cols_b] = (
+                part[k, 2, :, cols_b].astype(F32) + rs1[k, 1].astype(F32)
+            ).astype(BF)
+            rs_near_right(k, cols_b, 5).start()
+
+        @pl.when((step >= 4) & (step < nz + 4))
+        def _():
+            k = step - 4
+            for copy in rs_copies(k)[2:]:
+                copy.wait_recv()
+            total = (
+                part[k, 0].astype(F32) + rs2[k, 0].astype(F32) + rs2[k, 1].astype(F32)
+            ).astype(BF)
+            ret_out[k] = to_blocks(total)
+
+            @pl.when(k == 0)
+            def _():
+                ret_in[0, p_me] = ret_out[0, p_me]
+
+            to_plane(k, give_back)
+
+        @pl.when(step >= 5)
+        def _():
+            kk = mirror(step - 5)
+            wait_plane(kk, ret_in, r_recv)
+            ret_rows[kk] = to_rows(ret_in[kk])
+
+    e_lanes = lax.broadcasted_iota(jnp.int32, (tok, n_exp), 1)
+    ohc0 = e_lanes == routes_ref[:, 0:1]
+    ohc1 = e_lanes == routes_ref[:, 1:2]
+    crank0 = dot(before, one_hot(ohc0))
+    crank1 = dot(before, one_hot(ohc1)) + jnp.sum(
+        jnp.where(ohc0, 1.0, 0.0), axis=0, keepdims=True
+    )
+    cbase = base_of(e_lanes).astype(F32)
+    at0 = jnp.sum(jnp.where(ohc0, cbase + crank0, 0.0), axis=1, keepdims=True).astype(jnp.int32)
+    at1 = jnp.sum(jnp.where(ohc1, cbase + crank1, 0.0), axis=1, keepdims=True).astype(jnp.int32)
+    lanes = lax.broadcasted_iota(jnp.int32, (tok, nz * ROWS), 1)
+    take = jnp.concatenate([one_hot(lanes == at0), one_hot(lanes == at1)], axis=0)
+    square = jnp.zeros((tok, 1), F32)
+    block = min(512, width)
+    for c in range(width // block):
+        columns = slice(c * block, (c + 1) * block)
+        both = dot(take, ret_rows[:, :, columns].reshape(nz * ROWS, block))
+        mixed = rw_ref[:, 0:1] * both[:tok] + rw_ref[:, 1:2] * both[tok:]
+        combined[:, columns] = mixed
+        square = square + jnp.sum(mixed * mixed, axis=1, keepdims=True)
+    scale = lax.rsqrt(square / width + norm_eps)
+    out_ref[...] = (combined[...] * scale * fg_ref[...]).astype(BF)
+
+    @pl.loop(0, nz)
+    def _(k):
+        wait_plane(k, outgoing, d_send)
+        wait_plane(k, ret_out, r_send)
+        ag_right(k).wait_send()
+        ag_left(k).wait_send()
+        fwd_right(k).wait_send()
+        fwd_left(k).wait_send()
+        for copy in rs_copies(k):
+            copy.wait_send()
+
+
+def permutation():
+    source, piece, rank = np.meshgrid(
+        np.arange(PL), np.arange(SUB), np.arange(CAP), indexing="ij"
+    )
+    travel = (source * SUB + piece) * CAP + rank
+    rowwise = (piece * PL + source) * CAP + rank
+    matrix = np.zeros((PL * ROWS, PL * ROWS), np.float32)
+    matrix[rowwise.reshape(-1), travel.reshape(-1)] = 1.0
+    return matrix
+
+
 def expert_half(expert_in, routes, route_weights, expert_gain, gate_w, up_w, down_w, ffn_out_gain):
-    tok_rows = expert_in.shape[0]
-    model_width = expert_in.shape[1]
-    top_count = routes.shape[1]
-    expert_count = lax.axis_size(EP)
-    capacity = max(2, (3 * tok_rows * top_count + 2 * expert_count - 1) // (2 * expert_count))
-    normed = rms_scale(expert_in.astype(jnp.float32), expert_gain).astype(jnp.bfloat16)
-    pair_expert = routes.reshape(-1)
-    pair_count = pair_expert.shape[0]
-    one_hot = (pair_expert[:, None] == jnp.arange(expert_count, dtype=jnp.int32)[None, :]).astype(
-        jnp.int32
-    )
-    pair_rank = jnp.sum(jnp.cumsum(one_hot, axis=0) * one_hot, axis=1) - 1
-    pair_slot = pair_expert * capacity + pair_rank
-    slot_pair = (
-        jnp.full((expert_count * capacity,), pair_count, jnp.int32)
-        .at[pair_slot]
-        .set(jnp.arange(pair_count, dtype=jnp.int32))
-    )
-    padded = jnp.concatenate([normed, jnp.zeros((1, model_width), jnp.bfloat16)], axis=0)
-    outgoing = padded[slot_pair // top_count].reshape(expert_count, capacity, model_width)
-    gate_local = gate_w[0]
-    up_local = up_w[0]
-    down_local = down_w[0]
-    arrived = lax.all_to_all(outgoing, EP, split_axis=0, concat_axis=0, tiled=True)
-    flat_rows = arrived.reshape(-1, model_width)
-    shard_rows = lax.all_gather(flat_rows, "tp", axis=0, tiled=True)
-    hidden = clamped_unit(
-        jnp.dot(shard_rows, gate_local, preferred_element_type=jnp.float32),
-        jnp.dot(shard_rows, up_local, preferred_element_type=jnp.float32),
-    )
-    selected = lax.slice_in_dim(hidden, 0, flat_rows.shape[0] * lax.axis_size("tp"), axis=0)
-    result = summed_on_arrival(
-        jnp.dot(selected, down_local, preferred_element_type=jnp.float32).astype(jnp.bfloat16),
-        "tp",
-        0,
-    )
-    finished = result.astype(jnp.bfloat16).reshape(arrived.shape)
-    returned = lax.all_to_all(finished, EP, split_axis=0, concat_axis=0, tiled=True)
-    pair_result = returned.reshape(-1, model_width)[pair_slot].reshape(
-        tok_rows, top_count, model_width
-    )
-    combined = jnp.einsum("tk,tkd->td", route_weights, pair_result.astype(jnp.float32))
-    return rms_scale(combined, ffn_out_gain).astype(jnp.bfloat16)
+    nz = lax.axis_size("ep_0")
+    tok, width = expert_in.shape
+    ff = gate_w.shape[2]
+    matrix = permutation()
+    pin = jnp.asarray(matrix, BF)
+    pout = jnp.asarray(matrix.T, BF)
+    vmem = pl.BlockSpec(memory_space=pltpu.VMEM)
+    hbm = pl.BlockSpec(memory_space=pl.ANY)
+    travel = (nz, PL, ROWS, width // SUB)
+    dma = pltpu.SemaphoreType.DMA
+    return pl.pallas_call(
+        functools.partial(experts_kernel, nz),
+        out_shape=jax.ShapeDtypeStruct((tok, width), BF),
+        in_specs=[vmem] * 8 + [hbm] * 3,
+        out_specs=vmem,
+        scratch_shapes=[
+            pltpu.VMEM((tok, width), BF),
+            pltpu.VMEM(travel, BF),
+            pltpu.VMEM(travel, BF),
+            pltpu.VMEM((nz, 4, ROWS, width), BF),
+            pltpu.VMEM((nz, 4, ROWS, width), BF),
+            pltpu.VMEM((nz, 2, ROWS, width // 2), BF),
+            pltpu.VMEM((nz, 2, ROWS, width), BF),
+            pltpu.VMEM(travel, BF),
+            pltpu.VMEM(travel, BF),
+            pltpu.VMEM((nz, ROWS, width), BF),
+            pltpu.VMEM((width, 2 * ff), BF),
+            pltpu.VMEM((ff, width), BF),
+            pltpu.VMEM((tok, width), F32),
+            dma((3,)),
+            dma((nz,)),
+            dma((nz,)),
+            dma((nz, 4)),
+            dma((nz, 4)),
+            dma((nz, 6)),
+            dma((nz, 2)),
+            dma((nz, 4)),
+            dma((nz,)),
+            dma((nz,)),
+        ],
+        compiler_params=pltpu.CompilerParams(
+            collective_id=0, has_side_effects=True, vmem_limit_bytes=60 * 2**20
+        ),
+        cost_estimate=pl.CostEstimate(
+            flops=60 * 10**9, bytes_accessed=8 * 2**20, transcendentals=0
+        ),
+        name="experts",
+    )(
+        expert_in,
+        routes,
+        routes.T,
+        route_weights,
+        expert_gain[None, :],
+        ffn_out_gain[None, :],
+        pin,
+        pout,
+        gate_w,
+        up_w,
+        down_w,
+    )
 
 
 def local(
@@ -200,15 +582,18 @@
     down_w,
     ffn_out_gain,
 ):
-    mixer_out = mixer_half(queries, keys, values, query_gain, key_gain, out_weight, mixer_gain)
     expert_out = expert_half(
         expert_in, routes, route_weights, expert_gain, gate_w, up_w, down_w, ffn_out_gain
     )
+    mixer_out = mixer_half(queries, keys, values, query_gain, key_gain, out_weight, mixer_gain)
     return (mixer_out, expert_out)
 
 
 def solution(mesh):
-    split = Mesh(mesh.devices.reshape(8, 4, 2, mesh.shape["tp"]), ("ep_0", "ep_1", "ep_2", "tp"))
+    split = Mesh(
+        mesh.devices.reshape(mesh.shape["ep"] // 8, 4, 2, mesh.shape["tp"]),
+        ("ep_0", "ep_1", "ep_2", "tp"),
+    )
     return jax.shard_map(
         local,
         mesh=split,

time: 386 us -> 393 us (1.018)
  Pallas kernels: 0 us -> 149 us
  waiting for transfers between devices: 193 us -> 108 us
  starting transfers between devices: 36.8 us -> 3.86 us
  local copies, waits for them, and re-layouts: 21.8 us -> 5.03 us
  other arithmetic: 26.9 us -> 15.8 us
  matrix products: 66.5 us -> 73.8 us
    pallas_call x0 -> x1, Pallas kernels: none -> 149 us  [expert_half(): pl.pallas_call(functools.partial(experts_kernel, nz), out_shape=jax.Shape...]
    all_to_all x2 -> x0, waiting for transfers between devices: 95.9 us -> none  [the longest x1 48.4 us: expert_half(): lax.all_to_all(finished, EP, split_axis=0, concat_axis=0, tiled=True)]
    all_gather x4, waiting for transfers between devices: 23.4 us -> 108 us  [whole_of(): nearer = lax.all_gather(array, axes[-1], axis=dim, tiled=True)]
    all_gather x1 -> x0, waiting for transfers between devices: 66.8 us -> none  [expert_half(): shard_rows = lax.all_gather(flat_rows, 'tp', axis=0, tiled=True)]
    all_to_all x2 -> x0, starting transfers between devices: 27.5 us -> none  [the longest x1 14.4 us: expert_half(): lax.all_to_all(outgoing, EP, split_axis=0, concat_axis=0, tiled=True)]
    dot_general x4 -> x1, matrix products: 26 us -> 1.46 us  [mixer_half(): jnp.dot(attended, out_weight, preferred_element_type=jnp.float32)]
    dot_general x12, matrix products: 20.1 us -> 38.9 us  [one_block(): jnp.einsum('qhgd,khd->hgqk', query_norm, key_block, preferred_element_typ...]
    dot_general x12, matrix products: 20.3 us -> 33.5 us  [one_block(): jnp.einsum('hgqk,khd->hgqd', expo.astype(jnp.bfloat16), value_block, pref...]
  transfers between devices with their start and end apart: 9 -> 5, of which waited for: 7 -> 4; matrix products, arithmetic and copies ran while one was open for 27% -> 1% of each run, Pallas kernels for 0% -> 38%
where the time goes in v1:
time: 393 us; the launch traced here: 392 us
  Pallas kernels  149 us (38%)
  waiting for transfers between devices  108 us (27%)
  matrix products  73.8 us (19%)
  blocking collectives  22.5 us (6%)
  other arithmetic  15.8 us (4%)
  between operations  14 us (4%)
  local copies, waits for them, and re-layouts  5.03 us (1%)
    pallas_call x1, Pallas kernels, expert_half(): pl.pallas_call(functools.partial(experts_kernel, nz), out_shape=jax.Shape...  149 us
    all_gather x4, waiting for transfers between devices, whole_of(): nearer = lax.all_gather(array, axes[-1], axis=dim, tiled=True)  108 us
    dot_general x12, matrix products, one_block(): jnp.einsum('qhgd,khd->hgqk', query_norm, key_block, preferred_element_typ...  38.9 us
    dot_general x12, matrix products, one_block(): jnp.einsum('hgqk,khd->hgqd', expo.astype(jnp.bfloat16), value_block, pref...  33.5 us
    all_gather x2, blocking collectives, whole_of(): nearer = lax.all_gather(array, axes[-1], axis=dim, tiled=True)  22.5 us
    reduce_sum x12, other arithmetic, one_block(): new_total = running_total * factor + jnp.sum(expo, axis=-1)  8.67 us
  transfers between devices with their start and end apart: 5, of which 4 were waited for; matrix products, arithmetic and copies ran while one was open for 1% of the time, Pallas kernels for 38%

profile of v1, /device:TPU:1, one launch (start us, length us, event | category | flops | bytes accessed | tf_op | source)
XLA Modules:
  0.0 392.2 jit_solution(17305606123213174376)
XLA Ops:
  10.2 11.7 %all_gather.18 = bf16[768,128]{1,0:T(8,128)(2,1)} all-gather(bf16[192,128]{1,0:T(8,128)(2,1)S(1)} %pad_maximum_fusion.1), channel_id=1, replica_groups=mesh['ep_0'=8,'ep_1'=4,'ep_2'=2,'tp'=4] {'ep_1'}, dimensions={0}, use_global_device_ids=true | all-gather | bytes 245760 | tf_op jit(solution)/shard_map/all_gather | solution.py:34
  21.9 10.8 %all_gather.21 = bf16[768,128]{1,0:T(8,128)(2,1)} all-gather(bf16[192,128]{1,0:T(8,128)(2,1)} %param.21), channel_id=1, replica_groups=mesh['ep_0'=8,'ep_1'=4,'ep_2'=2,'tp'=4] {'ep_1'}, dimensions={0}, use_global_device_ids=true | all-gather | bytes 245760 | tf_op jit(solution)/shard_map/all_gather | solution.py:34
  32.8 29.8 %all-gather.5.cloned.1.call-done = bf16[6144,128]{1,0:T(8,128)(2,1)} async-done(((bf16[768,128]{1,0:T(8,128)(2,1)}), bf16[6144,128]{1,0:T(8,128)(2,1)}) %all-gather.5.cloned.1.call-update) | async-done | bytes 1572880 | tf_op jit(solution)/shard_map/all_gather | solution.py:34
  62.7 39.9 %all-gather.9.cloned.1.call-done = bf16[6144,128]{1,0:T(8,128)(2,1)} async-done(((bf16[768,128]{1,0:T(8,128)(2,1)}), bf16[6144,128]{1,0:T(8,128)(2,1)}) %all-gather.9.cloned.1.call-update) | async-done | bytes 1572880 | tf_op jit(solution)/shard_map/all_gather | solution.py:34
  107.0 18.0 %all-gather.7.cloned.1.call-done = bf16[12288,128]{1,0:T(8,128)(2,1)} async-done(((bf16[6144,128]{1,0:T(8,128)(2,1)}), bf16[12288,128]{1,0:T(8,128)(2,1)}) %all-gather.7.cloned.1.call-update) | async-done | bytes 3145744 | tf_op jit(solution)/shard_map/all_gather | solution.py:34
  125.0 20.4 %all-gather.11.cloned.1.call-done = bf16[12288,128]{1,0:T(8,128)(2,1)} async-done(((bf16[6144,128]{1,0:T(8,128)(2,1)}), bf16[12288,128]{1,0:T(8,128)(2,1)}) %all-gather.11.cloned.1.call-update) | async-done | bytes 3145744 | tf_op jit(solution)/shard_map/all_gather | solution.py:34
  145.5 83.1 %while.15 = (s32[]{:T(128)}, f32[1,4,192]{2,1,0:T(4,128)S(1)}, f32[1,4,192]{2,1,0:T(4,128)S(1)}, f32[1,4,192,128]{3,2,1,0:T(8,128)S(1)}, bf16[12,1024,1,128]{3,1...) while((s32[]{:T(128)}, f32[1,4,192]{2,1,0:T(4,128)S(1)}, ...), condition=%wide.region_5.6_spmd.clone, body=%wide.region_2.5_spmd.clone.sunk | while | flops 409244160 | bytes 23577732 | solution.py:124
  145.5 3.2 bitcast_reduce_fusion.2
  148.7 2.8 fusion.67
  152.4 3.2 bitcast_reduce_fusion.2
  155.7 2.8 fusion.67
  159.3 3.2 bitcast_reduce_fusion.2
  162.6 2.8 fusion.67
  166.3 3.2 bitcast_reduce_fusion.2
  169.5 2.8 fusion.67
  173.2 3.2 bitcast_reduce_fusion.2
  176.4 2.8 fusion.67
  180.1 3.2 bitcast_reduce_fusion.2
  183.4 2.8 fusion.67
  187.0 3.2 bitcast_reduce_fusion.2
  190.3 2.8 fusion.67
  194.0 3.2 bitcast_reduce_fusion.2
  197.2 2.8 fusion.67
  200.9 3.2 bitcast_reduce_fusion.2
  204.1 2.8 fusion.67
  207.8 3.2 bitcast_reduce_fusion.2
  211.1 2.8 fusion.67
  214.7 3.2 bitcast_reduce_fusion.2
  221.7 3.2 bitcast_reduce_fusion.2
  224.9 2.8 fusion.67
  230.4 3.7 all-to-all-start
  234.1 148.6 %experts.1 = bf16[128,2048]{1,0:T(8,128)(2,1)} custom-call(bf16[128,2048]{1,0:T(8,128)(2,1)} %x_ref.1, s32[128,2]{1,0:T(8,128)} %copy.34.routes_ref, s32[2,128]{1,0:T(2,128)} %bitcast.117, f32[128,2]{1,0:T(8,128)} %copy.35.rw_ref, f32[1,2048]{1,0:T(1,128)} %bitcast.118, f32[1,2048]{1,0:T(1,128)} %bitcast.119, ...), custom_call_target="tpu_custom_call" | custom-call | flops 60000002048 | bytes 8388608 | tf_op jit(solution)/shard_map/experts/pallas_call | solution.py:516
  (122 shorter events, 25.3 us)
Async XLA Ops:
  7.2 221.8 %copy-start = (bf16[512,2048]{1,0:T(8,128)(2,1)S(1)}, bf16[512,2048]{1,0:T(8,128)(2,1)}, u32[]{:S(2)}) copy-start(bf16[512,2048]{1,0:T(8,128)(2,1)} %param.24) | copy-start | bytes 6291460
  7.2 95.5 %copy-start.2 = (bf16[192,512]{1,0:T(8,128)(2,1)S(1)}, bf16[192,512]{1,0:T(8,128)(2,1)}, u32[]{:S(2)}) copy-start(bf16[192,512]{1,0:T(8,128)(2,1)} %param.19) | copy-start | bytes 589828
  7.2 55.5 %all-gather.5.cloned.1.call-start = ((), (), s32[]{:S(2)}) async-start(), calls=%async_computation.1 | async-start | bytes 1769472 | tf_op jit(solution)/shard_map/all_gather | solution.py:34
  9.2 94.7 %copy-start.6 = (f32[128]{0:T(128)S(1)}, f32[128]{0:T(128)}, u32[]{:S(2)}) copy-start(f32[128]{0:T(128)} %param.22) | copy-start | bytes 1540
  21.9 80.7 %all-gather.9.cloned.1.call-start = ((), (), s32[]{:S(2)}) async-start(), calls=%async_computation.3 | async-start | bytes 1769472 | tf_op jit(solution)/shard_map/all_gather | solution.py:34
  32.8 92.3 %all-gather.7.cloned.1.call-start = ((), (), s32[]{:S(2)}) async-start(), calls=%async_computation.2 | async-start | bytes 4718592 | tf_op jit(solution)/shard_map/all_gather | solution.py:34
  62.7 82.8 %all-gather.11.cloned.1.call-start = ((), (), s32[]{:S(2)}) async-start(), calls=%async_computation.4 | async-start | bytes 4718592 | tf_op jit(solution)/shard_map/all_gather | solution.py:34
  102.8 2.7 copy-start.5
  102.8 3.5 copy-start.4
  148.7 2.9 copy-start.1
  155.6 2.9 copy-start.1
  162.6 2.9 copy-start.1
  169.5 2.9 copy-start.1
  176.4 2.9 copy-start.1
  183.4 2.9 copy-start.1
  190.3 2.9 copy-start.1
  197.2 2.9 copy-start.1
  204.1 2.9 copy-start.1
  211.1 2.9 copy-start.1
  218.0 2.9 copy-start.1
  224.9 2.9 copy-start.1
  230.4 152.3 %all-to-all-start = ((bf16[4,48,2048]{2,1,0:T(8,128)(2,1)}), bf16[4,48,2048]{2,1,0:T(8,128)(2,1)S(1)}, u32[]{:S(2)}, u32[]{:S(2)}) async-start(bf16[4,48,2048]{2,1,0:T(8,128)(2,1)} %bitcast.110), calls=%async_computation | async-start | bytes 1572864 | tf_op jit(solution)/shard_map/all_to_all | solution.py:45
  234.1 148.9 %copy-start.3 = (f32[2048]{0:T(1024)S(1)}, f32[2048]{0:T(1024)}, u32[]{:S(2)}) copy-start(f32[2048]{0:T(1024)} %param.25) | copy-start | bytes 24580
Sparse Core Ops, SparseCore 0:
  22.0 40.5 all-gather.4
  64.4 38.1 all-gather.8
  104.4 20.5 all-gather.6
  126.7 18.7 all-gather.10

commit v2 on v1

--- a/solution.py
+++ b/solution.py
@@ -10,7 +10,9 @@
 from jax.sharding import PartitionSpec as P
 
 HEAD = 128
+HEADS = 4
 GRID_W = 64
+TP = 4
 EP = ("ep_0", "ep_1", "ep_2")
 EP_TP = ("ep_0", "ep_1", "ep_2", "tp")
 MESH = pl.DeviceIdType.MESH
@@ -28,24 +30,6 @@
 ROWS = PL * CAP
 
 
-def whole_of(array, axes, dim):
-    if not axes:
-        return array
-    nearer = lax.all_gather(array, axes[-1], axis=dim, tiled=True)
-    return whole_of(nearer, axes[:-1], dim)
-
-
-def in_blocks(array, dim, peers):
-    before, after = (array.shape[:dim], array.shape[dim + 1 :])
-    return jnp.moveaxis(array.reshape(*before, peers, -1, *after), dim, 0)
-
-
-def summed_on_arrival(array, axis, dim):
-    blocks = in_blocks(array, dim, lax.axis_size(axis))
-    arrived = lax.all_to_all(blocks, axis, split_axis=0, concat_axis=0, tiled=True)
-    return arrived.astype(jnp.float32).sum(axis=0)
-
-
 def rms_scale(values_in, gain):
     return (
         values_in
@@ -54,87 +38,6 @@
     )
 
 
-def turn_pair(halfpart, cosine, sine):
-    first_part, second_part = jnp.split(halfpart, 2, axis=-1)
-    return jnp.concatenate(
-        [first_part * cosine - second_part * sine, second_part * cosine + first_part * sine],
-        axis=-1,
-    )
-
-
-def grid_rotate(field, position):
-    half_width = field.shape[-1] // 2
-    inverse = rope_base ** (-jnp.arange(0, half_width, 2, dtype=jnp.float32) / half_width)
-    grid_row = (position // GRID_W).astype(jnp.float32)
-    grid_col = (position % GRID_W).astype(jnp.float32)
-    row_angle = (grid_row[:, None] * inverse[None, :])[:, None, :]
-    col_angle = (grid_col[:, None] * inverse[None, :])[:, None, :]
-    return jnp.concatenate(
-        [
-            turn_pair(field[..., :half_width], jnp.cos(row_angle), jnp.sin(row_angle)),
-            turn_pair(field[..., half_width:], jnp.cos(col_angle), jnp.sin(col_angle)),
-        ],
-        axis=-1,
-    )
-
-
-def mixer_half(queries, keys, values, query_gain, key_gain, out_weight, mixer_gain):
-    local_rows = queries.shape[0]
-    kv_local = keys.shape[1] // HEAD
-    group_size = queries.shape[1] // HEAD // kv_local
-    position = lax.axis_index(EP) * local_rows + jnp.arange(local_rows, dtype=jnp.int32)
-    query_f = queries.astype(jnp.float32).reshape(local_rows, kv_local * group_size, HEAD)
-    query_norm = grid_rotate(rms_scale(query_f, query_gain), position).astype(jnp.bfloat16)
-    query_norm = query_norm.reshape(local_rows, kv_local, group_size, HEAD)
-    key_f = keys.astype(jnp.float32).reshape(local_rows, kv_local, HEAD)
-    key_norm = grid_rotate(rms_scale(key_f, key_gain), position).astype(jnp.bfloat16)
-    key_norm = key_norm.reshape(local_rows, kv_local * HEAD)
-    score_scale = HEAD ** (-0.5)
-    initial = (
-        jnp.full((kv_local, group_size, local_rows), -1e30, jnp.float32),
-        jnp.zeros((kv_local, group_size, local_rows), jnp.float32),
-        jnp.zeros((kv_local, group_size, local_rows, HEAD), jnp.float32),
-    )
-    key_piece = whole_of(key_norm, ("ep_2", "ep_0", "ep_1"), 0)
-    value_piece = whole_of(values, ("ep_2", "ep_0", "ep_1"), 0)
-    piece_rows = key_piece.shape[0]
-    block_rows = 1024
-    key_blocks = key_piece.reshape(piece_rows // block_rows, block_rows, kv_local, HEAD)
-    value_blocks = value_piece.reshape(piece_rows // block_rows, block_rows, kv_local, HEAD)
-
-    def one_block(state, blocks_in):
-        running_max, running_total, weighted = state
-        key_block, value_block = blocks_in
-        scores = (
-            jnp.einsum("qhgd,khd->hgqk", query_norm, key_block, preferred_element_type=jnp.float32)
-            * score_scale
-        )
-        new_max = jnp.maximum(running_max, jnp.max(scores, axis=-1))
-        factor = jnp.exp(running_max - new_max)
-        expo = jnp.exp(scores - new_max[..., None])
-        new_total = running_total * factor + jnp.sum(expo, axis=-1)
-        new_weighted = weighted * factor[..., None] + jnp.einsum(
-            "hgqk,khd->hgqd",
-            expo.astype(jnp.bfloat16),
-            value_block,
-            preferred_element_type=jnp.float32,
-        )
-        return ((new_max, new_total, new_weighted), None)
-
-    state_out, unused = lax.scan(one_block, initial, (key_blocks, value_blocks))
-    final_max, final_total, weighted = state_out
-    attended = (weighted / final_total[..., None]).astype(jnp.bfloat16)
-    attended = jnp.transpose(attended, (2, 0, 1, 3)).reshape(
-        local_rows, kv_local * group_size * HEAD
-    )
-    projected = summed_on_arrival(
-        jnp.dot(attended, out_weight, preferred_element_type=jnp.float32).astype(jnp.bfloat16),
-        "tp",
-        0,
-    )
-    return rms_scale(projected, mixer_gain).astype(jnp.bfloat16)
-
-
 def dot(a, b):
     return jnp.dot(a, b, preferred_element_type=F32)
 
@@ -143,7 +46,7 @@
     return jnp.where(cond, 1.0, 0.0).astype(BF)
 
 
-def experts_kernel(
+def layer_kernel(
     nz,
     x_ref,
     routes_ref,
@@ -153,9 +56,21 @@
     fg_ref,
     pin_ref,
     pout_ref,
+    q_ref,
+    k_ref,
+    v_ref,
+    qg_ref,
+    kg_ref,
+    mg_ref,
+    cos_row_ref,
+    sin_row_ref,
+    cos_col_ref,
+    sin_col_ref,
     gate_hbm,
     up_hbm,
     down_hbm,
+    ow_hbm,
+    mix_ref,
     out_ref,
     normed,
     outgoing,
@@ -170,6 +85,13 @@
     wgu,
     wd,
     combined,
+    ow,
+    kv,
+    q_s,
+    m_s,
+    l_s,
+    acc_s,
+    att_s,
     w_sem,
     d_send,
     d_recv,
@@ -180,12 +102,22 @@
     rs2_recv,
     r_send,
     r_recv,
+    kz_send,
+    kz_recv,
+    ky_send,
+    ky_recv,
+    kc_send,
+    kc_recv,
 ):
     z = lax.axis_index("ep_0")
     p_me = lax.axis_index("ep_1") * 2 + lax.axis_index("ep_2")
     x_me = lax.axis_index("tp")
     right = {"tp": lax.rem(x_me + 1, 4)}
     left = {"tp": lax.rem(x_me + 3, 4)}
+    y_me = lax.axis_index("ep_1")
+    y_up = {"ep_1": lax.rem(y_me + 1, 4)}
+    y_down = {"ep_1": lax.rem(y_me + 3, 4)}
+    other_core = {"ep_2": 1 - lax.axis_index("ep_2")}
     tok, width = x_ref.shape
     half = width // 2
     sub_w = width // SUB
@@ -221,12 +153,41 @@
         pltpu.make_async_copy(gate_hbm.at[0], wgu.at[:, pl.ds(0, ff)], w_sem.at[0]),
         pltpu.make_async_copy(up_hbm.at[0], wgu.at[:, pl.ds(ff, ff)], w_sem.at[1]),
         pltpu.make_async_copy(down_hbm.at[0], wd, w_sem.at[2]),
+        pltpu.make_async_copy(ow_hbm, ow, w_sem.at[3]),
     ]
     for copy in w_copies:
         copy.start()
 
     xf = x_ref[...].astype(F32)
     normed[...] = rms_scale(xf, eg_ref[...]).astype(BF)
+
+    grid_rows = k_ref.shape[0] // GRID_W
+    first_row = (z * PL + p_me) * grid_rows
+    cosine = jnp.concatenate(
+        [cos_row_ref[pl.ds(first_row + g, 1), :] + cos_col_ref[...] for g in range(grid_rows)],
+        axis=0,
+    )
+    sine = jnp.concatenate(
+        [sin_row_ref[pl.ds(first_row + g, 1), :] + sin_col_ref[...] for g in range(grid_rows)],
+        axis=0,
+    )
+    lane = lax.broadcasted_iota(jnp.int32, cosine.shape, 1)
+    first_of_pair = (lane & 32) == 0
+
+    def normed_and_turned(head, gain):
+        field = rms_scale(head.astype(F32), gain)
+        swapped = jnp.where(
+            first_of_pair, pltpu.roll(field, HEAD - 32, 1), pltpu.roll(field, 32, 1)
+        )
+        return (field * cosine + swapped * sine).astype(BF)
+
+    kv[0, 0, 0, 0] = normed_and_turned(k_ref[...], kg_ref[...])
+    kv[0, 0, 0, 1] = v_ref[...]
+    for h in range(HEADS):
+        q_s[h] = normed_and_turned(q_ref[:, h * HEAD : (h + 1) * HEAD], qg_ref[...])
+    m_s[...] = jnp.full(m_s.shape, -1e30, F32)
+    l_s[...] = jnp.zeros(l_s.shape, F32)
+    acc_s[...] = jnp.zeros(acc_s.shape, F32)
 
     def base_of(e):
         o = (lax.shift_right_logical(e, 3) - z + nz) & (nz - 1)
@@ -290,6 +251,70 @@
             device_id_type=MESH,
         )
 
+    def x_copy(src, dst, send, recv, to):
+        return pltpu.make_async_remote_copy(
+            src_ref=src, dst_ref=dst, send_sem=send, recv_sem=recv, device_id=to,
+            device_id_type=MESH,
+        )
+
+    def kv_plane(i):
+        return x_copy(
+            kv.at[0, 0, 0], kv.at[mirror(i), 0, 0], kz_send.at[i], kz_recv.at[mirror(i)],
+            {"ep_0": plane(i)},
+        )
+
+    def kv_up(k):
+        return x_copy(kv.at[k, 0, 0], kv.at[k, 0, 1], ky_send.at[k, 0], ky_recv.at[k, 0], y_up)
+
+    def kv_down(k):
+        return x_copy(kv.at[k, 0, 0], kv.at[k, 0, 2], ky_send.at[k, 1], ky_recv.at[k, 1], y_down)
+
+    def k_far(k):
+        return x_copy(
+            kv.at[k, 0, 1, 0], kv.at[k, 0, 3, 0], ky_send.at[k, 2], ky_recv.at[k, 2], y_up
+        )
+
+    def v_far(k):
+        return x_copy(
+            kv.at[k, 0, 2, 1], kv.at[k, 0, 3, 1], ky_send.at[k, 3], ky_recv.at[k, 3], y_down
+        )
+
+    def kv_across(k):
+        return x_copy(kv.at[k, 0], kv.at[k, 1], kc_send.at[k], kc_recv.at[k], other_core)
+
+    def attend(k):
+        keys = kv[k, :, :, 0].reshape(-1, HEAD)
+        vals = kv[k, :, :, 1].reshape(-1, HEAD)
+
+        @pl.loop(0, HEADS)
+        def _(h):
+            scores = lax.dot_general(
+                q_s[h], keys, (((1,), (1,)), ((), ())), preferred_element_type=F32
+            ) * HEAD ** (-0.5)
+            peak = jnp.maximum(m_s[h], jnp.max(scores, axis=1, keepdims=True))
+            fade = jnp.exp(m_s[h] - peak)
+            expo = jnp.exp(scores - peak[:, :1])
+            m_s[h] = peak
+            sums = l_s[h] * fade
+            for c in range(expo.shape[1] // HEAD):
+                sums = sums + expo[:, c * HEAD : (c + 1) * HEAD]
+            l_s[h] = sums
+            acc_s[h] = acc_s[h] * fade + dot(expo.astype(BF), vals)
+
+    def project():
+        for h in range(HEADS):
+            total = jnp.sum(l_s[h], axis=1, keepdims=True)
+            att_s[:, h * HEAD : (h + 1) * HEAD] = (acc_s[h] / total).astype(BF)
+        share = att_s.shape[0] // TP
+        ours = jnp.concatenate(
+            [
+                att_s[pl.ds(pl.multiple_of(lax.rem(x_me + o, TP) * share, share), share), :]
+                for o in (0, 3, 1, 2)
+            ],
+            axis=0,
+        )
+        return dot(ours, ow[...]).astype(BF).reshape(TP, share, width)
+
     def to_plane(i, make):
         @pl.when(i == 0)
         def _():
@@ -321,12 +346,8 @@
         if i == 0:
             arr[0, p_me] = outgoing[0, p_me]
         to_plane(jnp.int32(i), dispatch)
-
-    def x_copy(src, dst, send, recv, to):
-        return pltpu.make_async_remote_copy(
-            src_ref=src, dst_ref=dst, send_sem=send, recv_sem=recv, device_id=to,
-            device_id_type=MESH,
-        )
+        if i > 0:
+            kv_plane(jnp.int32(i)).start()
 
     cols_a, cols_b = pl.ds(0, half), pl.ds(half, half)
 
@@ -378,6 +399,17 @@
             rs_near_right(k, cols_b, 5),
         )
 
+    def rs_start(k):
+        rs_far_left(k).start()
+        rs_far_right(k).start()
+        rs_near_left(k, cols_b, 3).start()
+        rs_near_right(k, cols_a, 4).start()
+
+    def rs_total(k):
+        for copy in rs_copies(k)[2:]:
+            copy.wait_recv()
+        return part[k, 0].astype(F32) + rs2[k, 0].astype(F32) + rs2[k, 1].astype(F32)
+
     @pl.loop(0, nz + 5)
     def _(step):
         @pl.when(step < nz)
@@ -388,6 +420,13 @@
             ag_right(k).start()
             ag_left(k).start()
 
+            @pl.when(k > 0)
+            def _():
+                wait_bytes(kv.at[k, 0, 0], kz_recv.at[k])
+
+            kv_up(k).start()
+            kv_down(k).start()
+
         @pl.when((step >= 1) & (step < nz + 1))
         def _():
             k = step - 1
@@ -395,6 +434,10 @@
             fwd_right(k).start()
             ag_left(k).wait_recv()
             fwd_left(k).start()
+            kv_up(k).wait_recv()
+            k_far(k).start()
+            kv_down(k).wait_recv()
+            v_far(k).start()
 
         @pl.when((step >= 2) & (step < nz + 2))
         def _():
@@ -415,12 +458,12 @@
                 (up_cut + 1.0) * gate_cut * (1.0 / (1.0 + jnp.exp(-sigmoid_slope * gate_cut)))
             ).astype(BF)
             part[k] = dot(hidden, wd[...]).astype(BF).reshape(4, ROWS, width)
-            rs_far_left(k).start()
-            rs_far_right(k).start()
-            rs_near_left(k, cols_b, 3).start()
-            rs_near_right(k, cols_a, 4).start()
-
-        @pl.when((step >= 3) & (step < nz + 3))
+            rs_start(k)
+            k_far(k).wait_recv()
+            v_far(k).wait_recv()
+            kv_across(k).start()
+
+        @pl.when((step >= 3) & (step < nz + 4))
         def _():
             k = step - 3
             rs_far_left(k).wait_recv()
@@ -437,12 +480,7 @@
         @pl.when((step >= 4) & (step < nz + 4))
         def _():
             k = step - 4
-            for copy in rs_copies(k)[2:]:
-                copy.wait_recv()
-            total = (
-                part[k, 0].astype(F32) + rs2[k, 0].astype(F32) + rs2[k, 1].astype(F32)
-            ).astype(BF)
-            ret_out[k] = to_blocks(total)
+            ret_out[k] = to_blocks(rs_total(k).astype(BF))
 
             @pl.when(k == 0)
             def _():
@@ -455,6 +493,19 @@
             kk = mirror(step - 5)
             wait_plane(kk, ret_in, r_recv)
             ret_rows[kk] = to_rows(ret_in[kk])
+
+        @pl.when((step >= 3) & (step < nz + 3))
+        def _():
+            k = step - 3
+            kv_across(k).wait_recv()
+            attend(k)
+
+        @pl.when(step == nz + 2)
+        def _():
+            part[nz] = project()
+            rs_start(nz)
+
+    mix_ref[...] = rms_scale(rs_total(nz), mg_ref[...]).astype(BF)
 
     e_lanes = lax.broadcasted_iota(jnp.int32, (tok, n_exp), 1)
     ohc0 = e_lanes == routes_ref[:, 0:1]
@@ -487,6 +538,18 @@
         ag_left(k).wait_send()
         fwd_right(k).wait_send()
         fwd_left(k).wait_send()
+        kv_up(k).wait_send()
+        kv_down(k).wait_send()
+        k_far(k).wait_send()
+        v_far(k).wait_send()
+        kv_across(k).wait_send()
+
+        @pl.when(k > 0)
+        def _():
+            kv_plane(k).wait_send()
+
+    @pl.loop(0, nz + 1)
+    def _(k):
         for copy in rs_copies(k):
             copy.wait_send()
 
@@ -502,66 +565,27 @@
     return matrix
 
 
-def expert_half(expert_in, routes, route_weights, expert_gain, gate_w, up_w, down_w, ffn_out_gain):
-    nz = lax.axis_size("ep_0")
-    tok, width = expert_in.shape
-    ff = gate_w.shape[2]
-    matrix = permutation()
-    pin = jnp.asarray(matrix, BF)
-    pout = jnp.asarray(matrix.T, BF)
-    vmem = pl.BlockSpec(memory_space=pltpu.VMEM)
-    hbm = pl.BlockSpec(memory_space=pl.ANY)
-    travel = (nz, PL, ROWS, width // SUB)
-    dma = pltpu.SemaphoreType.DMA
-    return pl.pallas_call(
-        functools.partial(experts_kernel, nz),
-        out_shape=jax.ShapeDtypeStruct((tok, width), BF),
-        in_specs=[vmem] * 8 + [hbm] * 3,
-        out_specs=vmem,
-        scratch_shapes=[
-            pltpu.VMEM((tok, width), BF),
-            pltpu.VMEM(travel, BF),
-            pltpu.VMEM(travel, BF),
-            pltpu.VMEM((nz, 4, ROWS, width), BF),
-            pltpu.VMEM((nz, 4, ROWS, width), BF),
-            pltpu.VMEM((nz, 2, ROWS, width // 2), BF),
-            pltpu.VMEM((nz, 2, ROWS, width), BF),
-            pltpu.VMEM(travel, BF),
-            pltpu.VMEM(travel, BF),
-            pltpu.VMEM((nz, ROWS, width), BF),
-            pltpu.VMEM((width, 2 * ff), BF),
-            pltpu.VMEM((ff, width), BF),
-            pltpu.VMEM((tok, width), F32),
-            dma((3,)),
-            dma((nz,)),
-            dma((nz,)),
-            dma((nz, 4)),
-            dma((nz, 4)),
-            dma((nz, 6)),
-            dma((nz, 2)),
-            dma((nz, 4)),
-            dma((nz,)),
-            dma((nz,)),
-        ],
-        compiler_params=pltpu.CompilerParams(
-            collective_id=0, has_side_effects=True, vmem_limit_bytes=60 * 2**20
-        ),
-        cost_estimate=pl.CostEstimate(
-            flops=60 * 10**9, bytes_accessed=8 * 2**20, transcendentals=0
-        ),
-        name="experts",
-    )(
-        expert_in,
-        routes,
-        routes.T,
-        route_weights,
-        expert_gain[None, :],
-        ffn_out_gain[None, :],
-        pin,
-        pout,
-        gate_w,
-        up_w,
-        down_w,
+def turn_tables(rows):
+    quarter = HEAD // 4
+    inverse = rope_base ** (-np.arange(quarter, dtype=np.float64) / quarter)
+
+    def table(count, make, at):
+        angle = np.arange(count, dtype=np.float64)[:, None] * inverse[None, :]
+        out = np.zeros((count, HEAD), np.float32)
+        out[:, at : at + 2 * quarter] = make(angle)
+        return jnp.asarray(out)
+
+    def cosines(angle):
+        return np.concatenate([np.cos(angle), np.cos(angle)], axis=1)
+
+    def sines(angle):
+        return np.concatenate([-np.sin(angle), np.sin(angle)], axis=1)
+
+    return (
+        table(rows, cosines, 0),
+        table(rows, sines, 0),
+        table(GRID_W, cosines, HEAD // 2),
+        table(GRID_W, sines, HEAD // 2),
     )
 
 
@@ -582,11 +606,89 @@
     down_w,
     ffn_out_gain,
 ):
-    expert_out = expert_half(
-        expert_in, routes, route_weights, expert_gain, gate_w, up_w, down_w, ffn_out_gain
-    )
-    mixer_out = mixer_half(queries, keys, values, query_gain, key_gain, out_weight, mixer_gain)
-    return (mixer_out, expert_out)
+    nz = lax.axis_size("ep_0")
+    tok, width = expert_in.shape
+    ff = gate_w.shape[2]
+    seq = queries.shape[0]
+    tables = turn_tables(nz * PL * seq // GRID_W)
+    matrix = permutation()
+    pin = jnp.asarray(matrix, BF)
+    pout = jnp.asarray(matrix.T, BF)
+    vmem = pl.BlockSpec(memory_space=pltpu.VMEM)
+    hbm = pl.BlockSpec(memory_space=pl.ANY)
+    travel = (nz, PL, ROWS, width // SUB)
+    dma = pltpu.SemaphoreType.DMA
+    return pl.pallas_call(
+        functools.partial(layer_kernel, nz),
+        out_shape=(
+            jax.ShapeDtypeStruct((seq // TP, width), BF),
+            jax.ShapeDtypeStruct((tok, width), BF),
+        ),
+        in_specs=[vmem] * 18 + [hbm] * 4,
+        out_specs=(vmem, vmem),
+        scratch_shapes=[
+            pltpu.VMEM((tok, width), BF),
+            pltpu.VMEM(travel, BF),
+            pltpu.VMEM(travel, BF),
+            pltpu.VMEM((nz, 4, ROWS, width), BF),
+            pltpu.VMEM((nz + 1, 4, ROWS, width), BF),
+            pltpu.VMEM((nz + 1, 2, ROWS, width // 2), BF),
+            pltpu.VMEM((nz + 1, 2, ROWS, width), BF),
+            pltpu.VMEM(travel, BF),
+            pltpu.VMEM(travel, BF),
+            pltpu.VMEM((nz, ROWS, width), BF),
+            pltpu.VMEM((width, 2 * ff), BF),
+            pltpu.VMEM((ff, width), BF),
+            pltpu.VMEM((tok, width), F32),
+            pltpu.VMEM(out_weight.shape, BF),
+            pltpu.VMEM((nz, 2, 4, 2, seq, HEAD), BF),
+            pltpu.VMEM((HEADS, seq, HEAD), BF),
+            pltpu.VMEM((HEADS, seq, HEAD), F32),
+            pltpu.VMEM((HEADS, seq, HEAD), F32),
+            pltpu.VMEM((HEADS, seq, HEAD), F32),
+            pltpu.VMEM((seq, HEADS * HEAD), BF),
+            dma((4,)),
+            dma((nz,)),
+            dma((nz,)),
+            dma((nz, 4)),
+            dma((nz, 4)),
+            dma((nz + 1, 6)),
+            dma((nz + 1, 2)),
+            dma((nz + 1, 4)),
+            dma((nz,)),
+            dma((nz,)),
+            dma((nz,)),
+            dma((nz,)),
+            dma((nz, 4)),
+            dma((nz, 4)),
+            dma((nz,)),
+            dma((nz,)),
+        ],
+        compiler_params=pltpu.CompilerParams(
+            collective_id=0, has_side_effects=True, vmem_limit_bytes=62 * 2**20
+        ),
+        name="layer",
+    )(
+        expert_in,
+        routes,
+        routes.T,
+        route_weights,
+        expert_gain[None, :],
+        ffn_out_gain[None, :],
+        pin,
+        pout,
+        queries,
+        keys,
+        values,
+        query_gain[None, :],
+        key_gain[None, :],
+        mixer_gain[None, :],
+        *tables,
+        gate_w,
+        up_w,
+        down_w,
+        out_weight,
+    )
 
 
 def solution(mesh):

time: 393 us -> 167 us (0.42)
  waiting for transfers between devices: 108 us -> 0 us
  matrix products: 73.8 us -> 0 us
  blocking collectives: 22.5 us -> 0 us
  other arithmetic: 15.8 us -> 0 us
  between operations: 14 us -> 0.64 us
  Pallas kernels: 149 us -> 159 us
    all_gather x4 -> x0, waiting for transfers between devices: 108 us -> none  [whole_of(): nearer = lax.all_gather(array, axes[-1], axis=dim, tiled=True)]
    dot_general x25 -> x0, matrix products: 73.8 us -> none  [the longest x12 38.9 us: one_block(): jnp.einsum('qhgd,khd->hgqk', query_norm, key_block, preferred_element_typ...]
    all_gather x2 -> x0, blocking collectives: 22.5 us -> none  [whole_of(): nearer = lax.all_gather(array, axes[-1], axis=dim, tiled=True)]
    pallas_call x1, Pallas kernels: 149 us -> 159 us  [local(): pl.pallas_call(functools.partial(layer_kernel, nz), out_shape=(jax.ShapeD...]
    reduce_sum x16 -> x0, other arithmetic: 10.2 us -> none  [the longest x12 8.67 us: one_block(): new_total = running_total * factor + jnp.sum(expo, axis=-1)]
  transfers between devices with their start and end apart: 5 -> 0, of which waited for: 4 -> 0; matrix products, arithmetic and copies ran while one was open for 1% -> 0% of each run, Pallas kernels for 38% -> 0%
where the time goes in v2:
time: 167 us; the launch traced here: 166 us
  Pallas kernels  159 us (95%)
  local copies, waits for them, and re-layouts  6.32 us (4%)
    pallas_call x1, Pallas kernels, local(): pl.pallas_call(functools.partial(layer_kernel, nz), out_shape=(jax.ShapeD...  159 us
    unnamed x4, local copies, waits for them, and re-layouts  6.32 us

profile of v2, /device:TPU:1, one launch (start us, length us, event | category | flops | bytes accessed | tf_op | source)
XLA Modules:
  0.0 166.4 jit_solution(9365948936537552327)
XLA Ops:
  0.6 1.4 copy.24.rw_ref
  2.0 1.4 copy.23.routes_ref
  3.5 159.5 %layer.1 = (bf16[48,2048]{1,0:T(8,128)(2,1)}, bf16[128,2048]{1,0:T(8,128)(2,1)}) custom-call(bf16[128,2048]{1,0:T(8,128)(2,1)} %x_ref.1, s32[128,2]{1,0:T(8,128)} %copy.23.routes_ref, s32[2,128]{1,0:T(2,128)} %bitcast.9, f32[128,2]{1,0:T(8,128)} %copy.24.rw_ref, f32[1,2048]{1,0:T(1,128)} %bitcast.6, f32[1,2048]{1,0:T(1,128)} %bitcast.7, ...), custom_call_target="tpu_custom_call" | custom-call | tf_op jit(solution)/shard_map/layer/pallas_call | solution.py:621
  162.9 1.6 copy.27
  164.6 1.9 %copy.28 = bf16[128,2048]{1,0:T(8,128)(2,1)} copy(bf16[128,2048]{1,0:T(8,128)(2,1)} %get-tuple-element.5) | data formatting | bytes 1048576

commit v3 on v2

--- a/solution.py
+++ b/solution.py
@@ -13,6 +13,7 @@
 HEADS = 4
 GRID_W = 64
 TP = 4
+OPERANDS = 17
 EP = ("ep_0", "ep_1", "ep_2")
 EP_TP = ("ep_0", "ep_1", "ep_2", "tp")
 MESH = pl.DeviceIdType.MESH
@@ -28,6 +29,12 @@
 CAP = 6
 SUB = 8
 ROWS = PL * CAP
+AWAY = (0, 1, -3, 3, 4, -2, 2, -1)
+NZ = len(AWAY)
+FIRST = (0, 1, 2)
+LATER = {0: (3,), 1: (5,), 2: (4, 7), 3: (6,)}
+INDEX = [[a % NZ for a in AWAY].index(d) for d in range(NZ)]
+MIRROR = [INDEX[-a % NZ] for a in AWAY]
 
 
 def rms_scale(values_in, gain):
@@ -46,12 +53,30 @@
     return jnp.where(cond, 1.0, 0.0).astype(BF)
 
 
-def layer_kernel(
+def layer_kernel(nz, *refs):
+    ours = refs[:OPERANDS]
+    held = refs[OPERANDS + 6 : 2 * OPERANDS + 6]
+    sems = refs[-1]
+    copies = [
+        pltpu.make_async_copy(src, dst, sems.at[i])
+        for i, (src, dst) in enumerate(zip(ours, held))
+    ]
+    for copy in copies:
+        copy.start()
+
+    def operands_here():
+        for copy in copies:
+            copy.wait()
+
+    layer(nz, operands_here, *held, *refs[OPERANDS : OPERANDS + 6], *refs[2 * OPERANDS + 6 : -1])
+
+
+def layer(
     nz,
+    operands_here,
     x_ref,
-    routes_ref,
     routes_t_ref,
-    rw_ref,
+    rw_t_ref,
     eg_ref,
     fg_ref,
     pin_ref,
@@ -87,6 +112,7 @@
     combined,
     ow,
     kv,
+    side,
     q_s,
     m_s,
     l_s,
@@ -127,15 +153,17 @@
     def peer(zz, p):
         return {"ep_0": zz, "ep_1": p // 2, "ep_2": lax.rem(p, 2)}
 
-    def away(i):
-        return jnp.where(lax.rem(i, 2) == 1, (i + 1) // 2, -(i // 2))
+    def entry(values, i):
+        found = jnp.full(jnp.shape(i), values[0], jnp.int32)
+        for j in range(1, nz):
+            found = jnp.where(i == j, values[j], found)
+        return found
 
     def plane(i):
-        return lax.rem(z + away(i) + nz, nz)
+        return lax.rem(z + entry([a % nz for a in AWAY], i), nz)
 
     def mirror(i):
-        other = jnp.where(lax.rem(i, 2) == 1, i + 1, i - 1)
-        return jnp.where((i == 0) | (i == nz - 1), i, other)
+        return entry(MIRROR, i)
 
     barrier = pltpu.get_barrier_semaphore()
 
@@ -158,6 +186,7 @@
     for copy in w_copies:
         copy.start()
 
+    operands_here()
     xf = x_ref[...].astype(F32)
     normed[...] = rms_scale(xf, eg_ref[...]).astype(BF)
 
@@ -191,14 +220,12 @@
 
     def base_of(e):
         o = (lax.shift_right_logical(e, 3) - z + nz) & (nz - 1)
-        idx = jnp.where(o == 0, 0, jnp.where(o <= nz // 2, 2 * o - 1, 2 * (nz - o)))
-        return idx * ROWS + (e & 7) * CAP
+        return entry(INDEX, o) * ROWS + (e & 7) * CAP
 
     e_rows = lax.broadcasted_iota(jnp.int32, (n_exp, tok), 0)
     t_a = lax.broadcasted_iota(jnp.int32, (tok, tok), 0)
     t_b = lax.broadcasted_iota(jnp.int32, (tok, tok), 1)
     before_t = one_hot(t_a < t_b)
-    before = one_hot(t_b < t_a)
     oh0 = e_rows == routes_t_ref[0:1, :]
     oh1 = e_rows == routes_t_ref[1:2, :]
     rank0 = dot(one_hot(oh0), before_t)
@@ -206,12 +233,13 @@
         jnp.where(oh0, 1.0, 0.0), axis=1, keepdims=True
     )
     base = base_of(e_rows).astype(F32)
-    place0 = jnp.sum(jnp.where(oh0, base + rank0, 0.0), axis=0, keepdims=True).astype(jnp.int32)
-    place1 = jnp.sum(jnp.where(oh1, base + rank1, 0.0), axis=0, keepdims=True).astype(jnp.int32)
-    slots = lax.broadcasted_iota(jnp.int32, (nz * ROWS, tok), 0)
+    place0 = jnp.sum(jnp.where(oh0, base + rank0, 0.0), axis=0, keepdims=True)
+    place1 = jnp.sum(jnp.where(oh1, base + rank1, 0.0), axis=0, keepdims=True)
+    slots = lax.broadcasted_iota(jnp.int32, (nz * ROWS, tok), 0).astype(F32)
     pick = one_hot((slots == place0) | (slots == place1))
-
-    pl.semaphore_wait(barrier, n_exp - 1 + 2)
+    side[...] = jnp.concatenate(
+        [place0, place1, rw_t_ref[...], jnp.zeros((4, tok), F32)], axis=0
+    )
 
     def stack_pieces(rows):
         return jnp.concatenate(
@@ -257,11 +285,33 @@
             device_id_type=MESH,
         )
 
-    def kv_plane(i):
+    z_up = {"ep_0": lax.rem(z + 1, nz)}
+    z_down = {"ep_0": lax.rem(z + nz - 1, nz)}
+
+    def kv_z_up(k, to):
+        return x_copy(kv.at[k, 0, 0], kv.at[to, 0, 0], kz_send.at[to, 0], kz_recv.at[to, 0], z_up)
+
+    def kv_z_down(k, to):
         return x_copy(
-            kv.at[0, 0, 0], kv.at[mirror(i), 0, 0], kz_send.at[i], kz_recv.at[mirror(i)],
-            {"ep_0": plane(i)},
-        )
+            kv.at[k, 0, 0], kv.at[to, 0, 0], kz_send.at[to, 0], kz_recv.at[to, 0], z_down
+        )
+
+    last = nz - 1
+    k_z_far = x_copy(
+        kv.at[last - 2, 0, 0, 0], kv.at[last, 0, 0, 0], kz_send.at[last, 0], kz_recv.at[last, 0],
+        z_up,
+    )
+    v_z_far = x_copy(
+        kv.at[last - 1, 0, 0, 1], kv.at[last, 0, 0, 1], kz_send.at[last, 1], kz_recv.at[last, 1],
+        z_down,
+    )
+
+    def each_plane(group, act):
+        act(jnp.maximum(2 * group - 1, 0))
+
+        @pl.when((group >= 1) & (group < nz // 2))
+        def _():
+            act(2 * group)
 
     def kv_up(k):
         return x_copy(kv.at[k, 0, 0], kv.at[k, 0, 1], ky_send.at[k, 0], ky_recv.at[k, 0], y_up)
@@ -343,11 +393,17 @@
     for i in range(nz):
         rows = dot(pick[i * ROWS : (i + 1) * ROWS, :], normed[...]).astype(BF)
         outgoing[i] = to_blocks(rows)
-        if i == 0:
-            arr[0, p_me] = outgoing[0, p_me]
-        to_plane(jnp.int32(i), dispatch)
-        if i > 0:
-            kv_plane(jnp.int32(i)).start()
+    arr[0, p_me] = outgoing[0, p_me]
+
+    pl.semaphore_wait(barrier, n_exp - 1 + 2)
+    to_plane(jnp.int32(MIRROR[FIRST[0]]), dispatch)
+    kv_z_up(0, 1).start()
+    kv_z_down(0, 2).start()
+    kv_up(0).start()
+    kv_down(0).start()
+
+    for i in FIRST[1:]:
+        to_plane(jnp.int32(MIRROR[i]), dispatch)
 
     cols_a, cols_b = pl.ds(0, half), pl.ds(half, half)
 
@@ -410,7 +466,12 @@
             copy.wait_recv()
         return part[k, 0].astype(F32) + rs2[k, 0].astype(F32) + rs2[k, 1].astype(F32)
 
-    @pl.loop(0, nz + 5)
+    def take_back(j):
+        kk = mirror(j)
+        wait_plane(kk, ret_in, r_recv)
+        ret_rows[kk] = to_rows(ret_in[kk])
+
+    @pl.loop(0, nz + 4)
     def _(step):
         @pl.when(step < nz)
         def _():
@@ -419,14 +480,6 @@
             xall[k, 0] = to_rows(arr[k])
             ag_right(k).start()
             ag_left(k).start()
-
-            @pl.when(k > 0)
-            def _():
-                wait_bytes(kv.at[k, 0, 0], kz_recv.at[k])
-
-            kv_up(k).start()
-            kv_down(k).start()
-
         @pl.when((step >= 1) & (step < nz + 1))
         def _():
             k = step - 1
@@ -434,10 +487,6 @@
             fwd_right(k).start()
             ag_left(k).wait_recv()
             fwd_left(k).start()
-            kv_up(k).wait_recv()
-            k_far(k).start()
-            kv_down(k).wait_recv()
-            v_far(k).start()
 
         @pl.when((step >= 2) & (step < nz + 2))
         def _():
@@ -459,13 +508,8 @@
             ).astype(BF)
             part[k] = dot(hidden, wd[...]).astype(BF).reshape(4, ROWS, width)
             rs_start(k)
-            k_far(k).wait_recv()
-            v_far(k).wait_recv()
-            kv_across(k).start()
-
-        @pl.when((step >= 3) & (step < nz + 4))
-        def _():
-            k = step - 3
+
+        def pass_on(k):
             rs_far_left(k).wait_recv()
             part[k, 1, :, cols_a] = (
                 part[k, 1, :, cols_a].astype(F32) + rs1[k, 0].astype(F32)
@@ -477,7 +521,77 @@
             ).astype(BF)
             rs_near_right(k, cols_b, 5).start()
 
-        @pl.when((step >= 4) & (step < nz + 4))
+        @pl.when((step >= 3) & (step < nz + 3))
+        def _():
+            pass_on(step - 3)
+
+        @pl.when(step == nz + 1)
+        def _():
+            part[nz] = project()
+            rs_start(nz)
+
+        @pl.when((step >= 1) & (step < nz // 2))
+        def _():
+            below, above = 2 * step - 1, 2 * step
+            kv_z_up(0, below).wait_recv()
+            kv_z_down(0, above).wait_recv()
+
+            @pl.when(step < nz // 2 - 1)
+            def _():
+                kv_z_up(below, below + 2).start()
+                kv_z_down(above, above + 2).start()
+
+            @pl.when(step == nz // 2 - 1)
+            def _():
+                k_z_far.start()
+                v_z_far.start()
+
+            for j in (below, above):
+                kv_up(j).start()
+                kv_down(j).start()
+
+        @pl.when(step == nz // 2)
+        def _():
+            k_z_far.wait_recv()
+            v_z_far.wait_recv()
+            kv_up(last).start()
+            kv_down(last).start()
+
+        for at, chunks in LATER.items():
+
+            @pl.when(step == at)
+            def _(chunks=chunks):
+                for i in chunks:
+                    to_plane(jnp.int32(MIRROR[i]), dispatch)
+
+        @pl.when((step >= 1) & (step <= nz // 2 + 1))
+        def _():
+            def forward(j):
+                kv_up(j).wait_recv()
+                k_far(j).start()
+                kv_down(j).wait_recv()
+                v_far(j).start()
+
+            each_plane(step - 1, forward)
+
+        @pl.when((step >= 2) & (step <= nz // 2 + 2))
+        def _():
+            def across(j):
+                k_far(j).wait_recv()
+                v_far(j).wait_recv()
+                kv_across(j).start()
+
+            each_plane(step - 2, across)
+
+        @pl.when((step >= 3) & (step <= nz // 2 + 3))
+        def _():
+            def attend_to(j):
+                kv_across(j).wait_recv()
+                attend(j)
+
+            each_plane(step - 3, attend_to)
+
+        @pl.when(step >= 4)
         def _():
             k = step - 4
             ret_out[k] = to_blocks(rs_total(k).astype(BF))
@@ -488,43 +602,29 @@
 
             to_plane(k, give_back)
 
-        @pl.when(step >= 5)
-        def _():
-            kk = mirror(step - 5)
-            wait_plane(kk, ret_in, r_recv)
-            ret_rows[kk] = to_rows(ret_in[kk])
-
-        @pl.when((step >= 3) & (step < nz + 3))
-        def _():
-            k = step - 3
-            kv_across(k).wait_recv()
-            attend(k)
-
         @pl.when(step == nz + 2)
         def _():
-            part[nz] = project()
-            rs_start(nz)
+            pass_on(nz)
+
+        @pl.when(step >= nz - 1)
+        def _():
+            take_back(step - (nz - 1))
 
     mix_ref[...] = rms_scale(rs_total(nz), mg_ref[...]).astype(BF)
 
-    e_lanes = lax.broadcasted_iota(jnp.int32, (tok, n_exp), 1)
-    ohc0 = e_lanes == routes_ref[:, 0:1]
-    ohc1 = e_lanes == routes_ref[:, 1:2]
-    crank0 = dot(before, one_hot(ohc0))
-    crank1 = dot(before, one_hot(ohc1)) + jnp.sum(
-        jnp.where(ohc0, 1.0, 0.0), axis=0, keepdims=True
-    )
-    cbase = base_of(e_lanes).astype(F32)
-    at0 = jnp.sum(jnp.where(ohc0, cbase + crank0, 0.0), axis=1, keepdims=True).astype(jnp.int32)
-    at1 = jnp.sum(jnp.where(ohc1, cbase + crank1, 0.0), axis=1, keepdims=True).astype(jnp.int32)
-    lanes = lax.broadcasted_iota(jnp.int32, (tok, nz * ROWS), 1)
+    for j in (5, 6, 7):
+        take_back(jnp.int32(j))
+
+    columns_of = side[...].T
+    at0, at1, weight0, weight1 = (columns_of[:, c : c + 1] for c in range(4))
+    lanes = lax.broadcasted_iota(jnp.int32, (tok, nz * ROWS), 1).astype(F32)
     take = jnp.concatenate([one_hot(lanes == at0), one_hot(lanes == at1)], axis=0)
     square = jnp.zeros((tok, 1), F32)
     block = min(512, width)
     for c in range(width // block):
         columns = slice(c * block, (c + 1) * block)
         both = dot(take, ret_rows[:, :, columns].reshape(nz * ROWS, block))
-        mixed = rw_ref[:, 0:1] * both[:tok] + rw_ref[:, 1:2] * both[tok:]
+        mixed = weight0 * both[:tok] + weight1 * both[tok:]
         combined[:, columns] = mixed
         square = square + jnp.sum(mixed * mixed, axis=1, keepdims=True)
     scale = lax.rsqrt(square / width + norm_eps)
@@ -544,9 +644,12 @@
         v_far(k).wait_send()
         kv_across(k).wait_send()
 
-        @pl.when(k > 0)
-        def _():
-            kv_plane(k).wait_send()
+        @pl.when((k > 0) & (k < last))
+        def _():
+            kv_z_up(0, k).wait_send()
+
+    k_z_far.wait_send()
+    v_z_far.wait_send()
 
     @pl.loop(0, nz + 1)
     def _(k):
@@ -607,6 +710,7 @@
     ffn_out_gain,
 ):
     nz = lax.axis_size("ep_0")
+    assert nz == NZ
     tok, width = expert_in.shape
     ff = gate_w.shape[2]
     seq = queries.shape[0]
@@ -618,15 +722,33 @@
     hbm = pl.BlockSpec(memory_space=pl.ANY)
     travel = (nz, PL, ROWS, width // SUB)
     dma = pltpu.SemaphoreType.DMA
+    operands = (
+        expert_in,
+        routes.T,
+        route_weights.T,
+        expert_gain[None, :],
+        ffn_out_gain[None, :],
+        pin,
+        pout,
+        queries,
+        keys,
+        values,
+        query_gain[None, :],
+        key_gain[None, :],
+        mixer_gain[None, :],
+        *tables,
+    )
+    assert len(operands) == OPERANDS
     return pl.pallas_call(
         functools.partial(layer_kernel, nz),
         out_shape=(
             jax.ShapeDtypeStruct((seq // TP, width), BF),
             jax.ShapeDtypeStruct((tok, width), BF),
         ),
-        in_specs=[vmem] * 18 + [hbm] * 4,
+        in_specs=[hbm] * (OPERANDS + 4),
         out_specs=(vmem, vmem),
-        scratch_shapes=[
+        scratch_shapes=[pltpu.VMEM(a.shape, a.dtype) for a in operands]
+        + [
             pltpu.VMEM((tok, width), BF),
             pltpu.VMEM(travel, BF),
             pltpu.VMEM(travel, BF),
@@ -642,6 +764,7 @@
             pltpu.VMEM((tok, width), F32),
             pltpu.VMEM(out_weight.shape, BF),
             pltpu.VMEM((nz, 2, 4, 2, seq, HEAD), BF),
+            pltpu.VMEM((8, tok), F32),
             pltpu.VMEM((HEADS, seq, HEAD), BF),
             pltpu.VMEM((HEADS, seq, HEAD), F32),
             pltpu.VMEM((HEADS, seq, HEAD), F32),
@@ -657,33 +780,20 @@
             dma((nz + 1, 4)),
             dma((nz,)),
             dma((nz,)),
-            dma((nz,)),
-            dma((nz,)),
+            dma((nz, 2)),
+            dma((nz, 2)),
             dma((nz, 4)),
             dma((nz, 4)),
             dma((nz,)),
             dma((nz,)),
+            dma((OPERANDS,)),
         ],
         compiler_params=pltpu.CompilerParams(
             collective_id=0, has_side_effects=True, vmem_limit_bytes=62 * 2**20
         ),
         name="layer",
     )(
-        expert_in,
-        routes,
-        routes.T,
-        route_weights,
-        expert_gain[None, :],
-        ffn_out_gain[None, :],
-        pin,
-        pout,
-        queries,
-        keys,
-        values,
-        query_gain[None, :],
-        key_gain[None, :],
-        mixer_gain[None, :],
-        *tables,
+        *operands,
         gate_w,
         up_w,
         down_w,

time: 167 us -> 146 us (0.87)
  Pallas kernels: 159 us -> 141 us
  local copies, waits for them, and re-layouts: 6.32 us -> 3.5 us
    pallas_call x1, Pallas kernels: 159 us -> 141 us  [local(): pl.pallas_call(functools.partial(layer_kernel, nz), out_shape=(jax.ShapeD...]
    unnamed x4 -> x2, local copies, waits for them, and re-layouts: 6.32 us -> 3.5 us
where the time goes in v3:
time: 146 us
  Pallas kernels  141 us (97%)
  local copies, waits for them, and re-layouts  3.5 us (2%)
    pallas_call x1, Pallas kernels, local(): pl.pallas_call(functools.partial(layer_kernel, nz), out_shape=(jax.ShapeD...  141 us
    unnamed x2, local copies, waits for them, and re-layouts  3.5 us

profile of v3, /device:TPU:1, one launch (start us, length us, event | category | flops | bytes accessed | tf_op | source)
XLA Modules:
  0.0 145.5 jit_solution(4609682368298148295)
XLA Ops:
  0.6 141.4 %layer.1 = (bf16[48,2048]{1,0:T(8,128)(2,1)}, bf16[128,2048]{1,0:T(8,128)(2,1)}) custom-call(bf16[128,2048]{1,0:T(8,128)(2,1)} %refs_0_.1, s32[2,128]{1,0:T(2,128)} %bitcast.10, f32[2,128]{1,0:T(2,128)} %bitcast.11, f32[1,2048]{1,0:T(1,128)} %bitcast.7, f32[1,2048]{1,0:T(1,128)} %bitcast.8, bf16[384,384]{1,0:T(8,128)(2,1)} %constant.14.clone.refs_5_.refs_6_, ...), custom_call_target="tpu_custom_call" | custom-call | tf_op jit(solution)/shard_map/layer/pallas_call | solution.py:742
  142.0 1.6 %copy.25 = bf16[48,2048]{1,0:T(8,128)(2,1)} copy(bf16[48,2048]{1,0:T(8,128)(2,1)} %get-tuple-element.4) | data formatting | bytes 393216
  143.6 1.9 %copy.26 = bf16[128,2048]{1,0:T(8,128)(2,1)} copy(bf16[128,2048]{1,0:T(8,128)(2,1)} %get-tuple-element.5) | data formatting | bytes 1048576

commit v4 on v3

--- a/solution.py
+++ b/solution.py
@@ -29,10 +29,10 @@
 CAP = 6
 SUB = 8
 ROWS = PL * CAP
-AWAY = (0, 1, -3, 3, 4, -2, 2, -1)
+AWAY = (0, 1, -3, 3, -2, 4, 2, -1)
 NZ = len(AWAY)
-FIRST = (0, 1, 2)
-LATER = {0: (3,), 1: (5,), 2: (4, 7), 3: (6,)}
+FIRST = (1, 2)
+LATER = {0: (3,), 1: (4,), 2: (5, 7), 3: (6,)}
 INDEX = [[a % NZ for a in AWAY].index(d) for d in range(NZ)]
 MIRROR = [INDEX[-a % NZ] for a in AWAY]
 
@@ -151,7 +151,7 @@
     n_exp = nz * PL
 
     def peer(zz, p):
-        return {"ep_0": zz, "ep_1": p // 2, "ep_2": lax.rem(p, 2)}
+        return {"ep_0": zz, "ep_1": lax.div(p, 2), "ep_2": lax.rem(p, 2)}
 
     def entry(values, i):
         found = jnp.full(jnp.shape(i), values[0], jnp.int32)
@@ -167,15 +167,19 @@
 
     barrier = pltpu.get_barrier_semaphore()
 
-    @pl.loop(1, n_exp)
-    def _(j):
-        to = lax.rem(z * PL + p_me + j, n_exp)
-        pl.semaphore_signal(
-            barrier, inc=1, device_id=peer(to // PL, lax.rem(to, PL)), device_id_type=MESH
-        )
-
-    pl.semaphore_signal(barrier, inc=1, device_id=left, device_id_type=MESH)
-    pl.semaphore_signal(barrier, inc=1, device_id=right, device_id_type=MESH)
+    def greet(device):
+        pl.semaphore_signal(barrier, inc=1, device_id=device, device_id_type=MESH)
+
+    greet(left)
+    greet(right)
+    for j in range(1, PL):
+        greet(peer(z, lax.rem(p_me + j, PL)))
+
+    @pl.loop(1, nz)
+    def _(d):
+        zz = lax.rem(z + d, nz)
+        for j in range(PL):
+            greet(peer(zz, lax.rem(p_me + j, PL)))
 
     w_copies = [
         pltpu.make_async_copy(gate_hbm.at[0], wgu.at[:, pl.ds(0, ff)], w_sem.at[0]),
@@ -189,34 +193,6 @@
     operands_here()
     xf = x_ref[...].astype(F32)
     normed[...] = rms_scale(xf, eg_ref[...]).astype(BF)
-
-    grid_rows = k_ref.shape[0] // GRID_W
-    first_row = (z * PL + p_me) * grid_rows
-    cosine = jnp.concatenate(
-        [cos_row_ref[pl.ds(first_row + g, 1), :] + cos_col_ref[...] for g in range(grid_rows)],
-        axis=0,
-    )
-    sine = jnp.concatenate(
-        [sin_row_ref[pl.ds(first_row + g, 1), :] + sin_col_ref[...] for g in range(grid_rows)],
-        axis=0,
-    )
-    lane = lax.broadcasted_iota(jnp.int32, cosine.shape, 1)
-    first_of_pair = (lane & 32) == 0
-
-    def normed_and_turned(head, gain):
-        field = rms_scale(head.astype(F32), gain)
-        swapped = jnp.where(
-            first_of_pair, pltpu.roll(field, HEAD - 32, 1), pltpu.roll(field, 32, 1)
-        )
-        return (field * cosine + swapped * sine).astype(BF)
-
-    kv[0, 0, 0, 0] = normed_and_turned(k_ref[...], kg_ref[...])
-    kv[0, 0, 0, 1] = v_ref[...]
-    for h in range(HEADS):
-        q_s[h] = normed_and_turned(q_ref[:, h * HEAD : (h + 1) * HEAD], qg_ref[...])
-    m_s[...] = jnp.full(m_s.shape, -1e30, F32)
-    l_s[...] = jnp.zeros(l_s.shape, F32)
-    acc_s[...] = jnp.zeros(acc_s.shape, F32)
 
     def base_of(e):
         o = (lax.shift_right_logical(e, 3) - z + nz) & (nz - 1)
@@ -263,7 +239,7 @@
         return pltpu.make_async_remote_copy(
             src_ref=outgoing.at[i, p],
             dst_ref=arr.at[mirror(i), p_me],
-            send_sem=d_send.at[i],
+            send_sem=d_send.at[jnp.minimum(i, 1)],
             recv_sem=d_recv.at[mirror(i)],
             device_id=peer(plane(i), p),
             device_id_type=MESH,
@@ -273,7 +249,7 @@
         return pltpu.make_async_remote_copy(
             src_ref=ret_out.at[i, p],
             dst_ref=ret_in.at[mirror(i), p_me],
-            send_sem=r_send.at[i],
+            send_sem=r_send.at[jnp.minimum(i, 1)],
             recv_sem=r_recv.at[mirror(i)],
             device_id=peer(plane(i), p),
             device_id_type=MESH,
@@ -289,20 +265,20 @@
     z_down = {"ep_0": lax.rem(z + nz - 1, nz)}
 
     def kv_z_up(k, to):
-        return x_copy(kv.at[k, 0, 0], kv.at[to, 0, 0], kz_send.at[to, 0], kz_recv.at[to, 0], z_up)
+        return x_copy(kv.at[k, 0, 0], kv.at[to, 0, 0], kz_send.at[0], kz_recv.at[to, 0], z_up)
 
     def kv_z_down(k, to):
         return x_copy(
-            kv.at[k, 0, 0], kv.at[to, 0, 0], kz_send.at[to, 0], kz_recv.at[to, 0], z_down
+            kv.at[k, 0, 0], kv.at[to, 0, 0], kz_send.at[0], kz_recv.at[to, 0], z_down
         )
 
     last = nz - 1
     k_z_far = x_copy(
-        kv.at[last - 2, 0, 0, 0], kv.at[last, 0, 0, 0], kz_send.at[last, 0], kz_recv.at[last, 0],
+        kv.at[last - 2, 0, 0, 0], kv.at[last, 0, 0, 0], kz_send.at[0], kz_recv.at[last, 0],
         z_up,
     )
     v_z_far = x_copy(
-        kv.at[last - 1, 0, 0, 1], kv.at[last, 0, 0, 1], kz_send.at[last, 1], kz_recv.at[last, 1],
+        kv.at[last - 1, 0, 0, 1], kv.at[last, 0, 0, 1], kz_send.at[0], kz_recv.at[last, 1],
         z_down,
     )
 
@@ -314,23 +290,23 @@
             act(2 * group)
 
     def kv_up(k):
-        return x_copy(kv.at[k, 0, 0], kv.at[k, 0, 1], ky_send.at[k, 0], ky_recv.at[k, 0], y_up)
+        return x_copy(kv.at[k, 0, 0], kv.at[k, 0, 1], ky_send.at[0], ky_recv.at[k, 0], y_up)
 
     def kv_down(k):
-        return x_copy(kv.at[k, 0, 0], kv.at[k, 0, 2], ky_send.at[k, 1], ky_recv.at[k, 1], y_down)
+        return x_copy(kv.at[k, 0, 0], kv.at[k, 0, 2], ky_send.at[0], ky_recv.at[k, 1], y_down)
 
     def k_far(k):
         return x_copy(
-            kv.at[k, 0, 1, 0], kv.at[k, 0, 3, 0], ky_send.at[k, 2], ky_recv.at[k, 2], y_up
+            kv.at[k, 0, 1, 0], kv.at[k, 0, 3, 0], ky_send.at[0], ky_recv.at[k, 2], y_up
         )
 
     def v_far(k):
         return x_copy(
-            kv.at[k, 0, 2, 1], kv.at[k, 0, 3, 1], ky_send.at[k, 3], ky_recv.at[k, 3], y_down
+            kv.at[k, 0, 2, 1], kv.at[k, 0, 3, 1], ky_send.at[0], ky_recv.at[k, 3], y_down
         )
 
     def kv_across(k):
-        return x_copy(kv.at[k, 0], kv.at[k, 1], kc_send.at[k], kc_recv.at[k], other_core)
+        return x_copy(kv.at[k, 0], kv.at[k, 1], kc_send.at[0], kc_recv.at[k], other_core)
 
     def attend(k):
         keys = kv[k, :, :, 0].reshape(-1, HEAD)
@@ -390,59 +366,94 @@
         def _():
             wait_bytes(ref.at[i], sem.at[i])
 
-    for i in range(nz):
+    def gather(i):
         rows = dot(pick[i * ROWS : (i + 1) * ROWS, :], normed[...]).astype(BF)
         outgoing[i] = to_blocks(rows)
+
+    gather(0)
+    pl.semaphore_wait(barrier, n_exp - 1 + 2)
+    to_plane(jnp.int32(0), dispatch)
     arr[0, p_me] = outgoing[0, p_me]
 
-    pl.semaphore_wait(barrier, n_exp - 1 + 2)
-    to_plane(jnp.int32(MIRROR[FIRST[0]]), dispatch)
+    for c in FIRST:
+        gather(MIRROR[c])
+        to_plane(jnp.int32(MIRROR[c]), dispatch)
+
+    grid_rows = k_ref.shape[0] // GRID_W
+    first_row = (z * PL + p_me) * grid_rows
+    cosine = jnp.concatenate(
+        [cos_row_ref[pl.ds(first_row + g, 1), :] + cos_col_ref[...] for g in range(grid_rows)],
+        axis=0,
+    )
+    sine = jnp.concatenate(
+        [sin_row_ref[pl.ds(first_row + g, 1), :] + sin_col_ref[...] for g in range(grid_rows)],
+        axis=0,
+    )
+    lane = lax.broadcasted_iota(jnp.int32, cosine.shape, 1)
+    first_of_pair = (lane & 32) == 0
+
+    def normed_and_turned(head, gain):
+        field = rms_scale(head.astype(F32), gain)
+        swapped = jnp.where(
+            first_of_pair, pltpu.roll(field, HEAD - 32, 1), pltpu.roll(field, 32, 1)
+        )
+        return (field * cosine + swapped * sine).astype(BF)
+
+    kv[0, 0, 0, 0] = normed_and_turned(k_ref[...], kg_ref[...])
+    kv[0, 0, 0, 1] = v_ref[...]
     kv_z_up(0, 1).start()
     kv_z_down(0, 2).start()
     kv_up(0).start()
     kv_down(0).start()
 
-    for i in FIRST[1:]:
-        to_plane(jnp.int32(MIRROR[i]), dispatch)
+    for c in range(1, nz):
+        if c not in FIRST:
+            gather(MIRROR[c])
+
+    for h in range(HEADS):
+        q_s[h] = normed_and_turned(q_ref[:, h * HEAD : (h + 1) * HEAD], qg_ref[...])
+    m_s[...] = jnp.full(m_s.shape, -1e30, F32)
+    l_s[...] = jnp.zeros(l_s.shape, F32)
+    acc_s[...] = jnp.zeros(acc_s.shape, F32)
 
     cols_a, cols_b = pl.ds(0, half), pl.ds(half, half)
 
     def ag_right(k):
-        return x_copy(xall.at[k, 0], xall.at[k, 1], ag_send.at[k, 0], ag_recv.at[k, 0], right)
+        return x_copy(xall.at[k, 0], xall.at[k, 1], ag_send.at[0], ag_recv.at[k, 0], right)
 
     def ag_left(k):
-        return x_copy(xall.at[k, 0], xall.at[k, 2], ag_send.at[k, 1], ag_recv.at[k, 1], left)
+        return x_copy(xall.at[k, 0], xall.at[k, 2], ag_send.at[0], ag_recv.at[k, 1], left)
 
     def fwd_right(k):
         return x_copy(
             xall.at[k, 1, :, cols_a], xall.at[k, 3, :, cols_a],
-            ag_send.at[k, 2], ag_recv.at[k, 2], right,
+            ag_send.at[0], ag_recv.at[k, 2], right,
         )
 
     def fwd_left(k):
         return x_copy(
             xall.at[k, 2, :, cols_b], xall.at[k, 3, :, cols_b],
-            ag_send.at[k, 3], ag_recv.at[k, 3], left,
+            ag_send.at[0], ag_recv.at[k, 3], left,
         )
 
     def rs_far_left(k):
         return x_copy(
-            part.at[k, 3, :, cols_a], rs1.at[k, 0], rs_send.at[k, 0], rs1_recv.at[k, 0], left
+            part.at[k, 3, :, cols_a], rs1.at[k, 0], rs_send.at[0], rs1_recv.at[k, 0], left
         )
 
     def rs_far_right(k):
         return x_copy(
-            part.at[k, 3, :, cols_b], rs1.at[k, 1], rs_send.at[k, 1], rs1_recv.at[k, 1], right
+            part.at[k, 3, :, cols_b], rs1.at[k, 1], rs_send.at[0], rs1_recv.at[k, 1], right
         )
 
     def rs_near_left(k, c, s):
         return x_copy(
-            part.at[k, 1, :, c], rs2.at[k, 1, :, c], rs_send.at[k, s], rs2_recv.at[k, s - 2], left
+            part.at[k, 1, :, c], rs2.at[k, 1, :, c], rs_send.at[0], rs2_recv.at[k, s - 2], left
         )
 
     def rs_near_right(k, c, s):
         return x_copy(
-            part.at[k, 2, :, c], rs2.at[k, 0, :, c], rs_send.at[k, s], rs2_recv.at[k, s - 2], right
+            part.at[k, 2, :, c], rs2.at[k, 0, :, c], rs_send.at[0], rs2_recv.at[k, s - 2], right
         )
 
     def rs_copies(k):
@@ -455,9 +466,11 @@
             rs_near_right(k, cols_b, 5),
         )
 
-    def rs_start(k):
+    def rs_far(k):
         rs_far_left(k).start()
         rs_far_right(k).start()
+
+    def rs_near(k):
         rs_near_left(k, cols_b, 3).start()
         rs_near_right(k, cols_a, 4).start()
 
@@ -507,7 +520,7 @@
                 (up_cut + 1.0) * gate_cut * (1.0 / (1.0 + jnp.exp(-sigmoid_slope * gate_cut)))
             ).astype(BF)
             part[k] = dot(hidden, wd[...]).astype(BF).reshape(4, ROWS, width)
-            rs_start(k)
+            rs_far(k)
 
         def pass_on(k):
             rs_far_left(k).wait_recv()
@@ -525,23 +538,27 @@
         def _():
             pass_on(step - 3)
 
-        @pl.when(step == nz + 1)
-        def _():
-            part[nz] = project()
-            rs_start(nz)
-
-        @pl.when((step >= 1) & (step < nz // 2))
-        def _():
-            below, above = 2 * step - 1, 2 * step
+        @pl.when((step >= 2) & (step < nz + 2))
+        def _():
+            rs_near(step - 2)
+
+        @pl.when(step == nz + 2)
+        def _():
+            rs_far(nz)
+            rs_near(nz)
+
+        @pl.when((step >= 2) & (step <= nz // 2))
+        def _():
+            below, above = 2 * step - 3, 2 * step - 2
             kv_z_up(0, below).wait_recv()
             kv_z_down(0, above).wait_recv()
 
-            @pl.when(step < nz // 2 - 1)
+            @pl.when(step < nz // 2)
             def _():
                 kv_z_up(below, below + 2).start()
                 kv_z_down(above, above + 2).start()
 
-            @pl.when(step == nz // 2 - 1)
+            @pl.when(step == nz // 2)
             def _():
                 k_z_far.start()
                 v_z_far.start()
@@ -550,7 +567,7 @@
                 kv_up(j).start()
                 kv_down(j).start()
 
-        @pl.when(step == nz // 2)
+        @pl.when(step == nz // 2 + 1)
         def _():
             k_z_far.wait_recv()
             v_z_far.wait_recv()
@@ -564,7 +581,7 @@
                 for i in chunks:
                     to_plane(jnp.int32(MIRROR[i]), dispatch)
 
-        @pl.when((step >= 1) & (step <= nz // 2 + 1))
+        @pl.when((step >= 2) & (step <= nz // 2 + 2))
         def _():
             def forward(j):
                 kv_up(j).wait_recv()
@@ -572,24 +589,24 @@
                 kv_down(j).wait_recv()
                 v_far(j).start()
 
-            each_plane(step - 1, forward)
-
-        @pl.when((step >= 2) & (step <= nz // 2 + 2))
+            each_plane(step - 2, forward)
+
+        @pl.when((step >= 3) & (step <= nz // 2 + 3))
         def _():
             def across(j):
                 k_far(j).wait_recv()
                 v_far(j).wait_recv()
                 kv_across(j).start()
 
-            each_plane(step - 2, across)
-
-        @pl.when((step >= 3) & (step <= nz // 2 + 3))
+            each_plane(step - 3, across)
+
+        @pl.when((step >= 4) & (step <= nz // 2 + 4))
         def _():
             def attend_to(j):
                 kv_across(j).wait_recv()
                 attend(j)
 
-            each_plane(step - 3, attend_to)
+            each_plane(step - 4, attend_to)
 
         @pl.when(step >= 4)
         def _():
@@ -602,7 +619,11 @@
 
             to_plane(k, give_back)
 
-        @pl.when(step == nz + 2)
+        @pl.when(step == nz)
+        def _():
+            part[nz] = project()
+
+        @pl.when(step == nz + 3)
         def _():
             pass_on(nz)
 
@@ -630,31 +651,32 @@
     scale = lax.rsqrt(square / width + norm_eps)
     out_ref[...] = (combined[...] * scale * fg_ref[...]).astype(BF)
 
-    @pl.loop(0, nz)
-    def _(k):
-        wait_plane(k, outgoing, d_send)
-        wait_plane(k, ret_out, r_send)
-        ag_right(k).wait_send()
-        ag_left(k).wait_send()
-        fwd_right(k).wait_send()
-        fwd_left(k).wait_send()
-        kv_up(k).wait_send()
-        kv_down(k).wait_send()
-        k_far(k).wait_send()
-        v_far(k).wait_send()
-        kv_across(k).wait_send()
-
-        @pl.when((k > 0) & (k < last))
-        def _():
-            kv_z_up(0, k).wait_send()
-
-    k_z_far.wait_send()
-    v_z_far.wait_send()
-
-    @pl.loop(0, nz + 1)
-    def _(k):
-        for copy in rs_copies(k):
-            copy.wait_send()
+    for blocks, sems in ((outgoing, d_send), (ret_out, r_send)):
+        wait_bytes(blocks.at[0, pl.ds(0, PL - 1)], sems.at[0])
+        wait_bytes(blocks.at[pl.ds(1, nz - 1)], sems.at[1])
+    wait_bytes(xall.at[:, pl.ds(0, 3)], ag_send.at[0])
+    wait_bytes(part.at[:, pl.ds(0, 3)], rs_send.at[0])
+    wait_bytes(kv.at[pl.ds(0, nz - 1), 0, 0], kz_send.at[0])
+    wait_bytes(kv.at[:, 0, pl.ds(0, 3)], ky_send.at[0])
+    wait_bytes(kv.at[:, 0], kc_send.at[0])
+
+
+def hand_over(mix_hbm, rows_hbm, mix_out, rows_out, mix_v, rows_v, sems):
+    taken = [
+        pltpu.make_async_copy(mix_hbm, mix_v, sems.at[0]),
+        pltpu.make_async_copy(rows_hbm, rows_v, sems.at[1]),
+    ]
+    given = [
+        pltpu.make_async_copy(mix_v, mix_out, sems.at[2]),
+        pltpu.make_async_copy(rows_v, rows_out, sems.at[3]),
+    ]
+    for copy in taken:
+        copy.start()
+    for here, there in zip(taken, given):
+        here.wait()
+        there.start()
+    for copy in given:
+        copy.wait()
 
 
 def permutation():
@@ -739,7 +761,7 @@
         *tables,
     )
     assert len(operands) == OPERANDS
-    return pl.pallas_call(
+    made = pl.pallas_call(
         functools.partial(layer_kernel, nz),
         out_shape=(
             jax.ShapeDtypeStruct((seq // TP, width), BF),
@@ -771,20 +793,20 @@
             pltpu.VMEM((HEADS, seq, HEAD), F32),
             pltpu.VMEM((seq, HEADS * HEAD), BF),
             dma((4,)),
+            dma((2,)),
             dma((nz,)),
-            dma((nz,)),
+            dma((1,)),
             dma((nz, 4)),
-            dma((nz, 4)),
-            dma((nz + 1, 6)),
+            dma((1,)),
             dma((nz + 1, 2)),
             dma((nz + 1, 4)),
+            dma((2,)),
             dma((nz,)),
-            dma((nz,)),
+            dma((1,)),
             dma((nz, 2)),
-            dma((nz, 2)),
+            dma((1,)),
             dma((nz, 4)),
-            dma((nz, 4)),
-            dma((nz,)),
+            dma((1,)),
             dma((nz,)),
             dma((OPERANDS,)),
         ],
@@ -798,6 +820,16 @@
         up_w,
         down_w,
         out_weight,
+    )
+    return tuple(
+        pl.pallas_call(
+            hand_over,
+            out_shape=tuple(jax.ShapeDtypeStruct(a.shape, a.dtype) for a in made),
+            in_specs=[hbm] * 2,
+            out_specs=(hbm, hbm),
+            scratch_shapes=[pltpu.VMEM(a.shape, a.dtype) for a in made] + [dma((4,))],
+            name="hand_over",
+        )(*made)
     )
 
 

time: 146 us -> 140 us (0.959)
  local copies, waits for them, and re-layouts: 3.5 us -> 0 us
  Pallas kernels: 141 us -> 138 us
    pallas_call x1, Pallas kernels: 141 us -> 137 us  [local(): pl.pallas_call(functools.partial(layer_kernel, nz), out_shape=(jax.ShapeD...]
    unnamed x2 -> x0, local copies, waits for them, and re-layouts: 3.5 us -> none
    pallas_call x0 -> x1, Pallas kernels: none -> 1.98 us  [local(): pl.pallas_call(hand_over, out_shape=tuple((jax.ShapeDtypeStruct(a.shape,...]
where the time goes in v4:
time: 140 us; the launch traced here: 139 us
  Pallas kernels  138 us (99%)
    pallas_call x1, Pallas kernels, local(): pl.pallas_call(functools.partial(layer_kernel, nz), out_shape=(jax.ShapeD...  137 us

profile of v4, /device:TPU:1, one launch (start us, length us, event | category | flops | bytes accessed | tf_op | source)
XLA Modules:
  0.0 139.1 jit_solution(12993201792059893249)
XLA Ops:
  0.6 136.5 %layer.1 = (bf16[48,2048]{1,0:T(8,128)(2,1)}, bf16[128,2048]{1,0:T(8,128)(2,1)}) custom-call(bf16[128,2048]{1,0:T(8,128)(2,1)} %refs_0_.1, s32[2,128]{1,0:T(2,128)} %bitcast.10, f32[2,128]{1,0:T(2,128)} %bitcast.11, f32[1,2048]{1,0:T(1,128)} %bitcast.7, f32[1,2048]{1,0:T(1,128)} %bitcast.8, bf16[384,384]{1,0:T(8,128)(2,1)} %constant.14.clone.refs_5_.refs_6_, ...), custom_call_target="tpu_custom_call" | custom-call | tf_op jit(solution)/shard_map/layer/pallas_call | solution.py:764
  137.1 2.0 %hand_over.1 = (bf16[48,2048]{1,0:T(8,128)(2,1)}, bf16[128,2048]{1,0:T(8,128)(2,1)}) custom-call(bf16[48,2048]{1,0:T(8,128)(2,1)} %get-tuple-element.4.mix_hbm, bf16[128,2048]{1,0:T(8,128)(2,1)} %get-tuple-element.5.rows_hbm), custom_call_target="tpu_custom_call" | custom-call | tf_op jit(solution)/shard_map/hand_over/pallas_call | solution.py:825

commit v5 on v4

--- a/solution.py
+++ b/solution.py
@@ -29,10 +29,10 @@
 CAP = 6
 SUB = 8
 ROWS = PL * CAP
-AWAY = (0, 1, -3, 3, -2, 4, 2, -1)
+AWAY = (0, 1, -2, 3, 4, -3, 2, -1)
 NZ = len(AWAY)
-FIRST = (1, 2)
-LATER = {0: (3,), 1: (4,), 2: (5, 7), 3: (6,)}
+FIRST = (1, 2, 3)
+LATER = {0: (4,), 2: (5,), 3: (6, 7)}
 INDEX = [[a % NZ for a in AWAY].index(d) for d in range(NZ)]
 MIRROR = [INDEX[-a % NZ] for a in AWAY]
 
@@ -479,6 +479,36 @@
             copy.wait_recv()
         return part[k, 0].astype(F32) + rs2[k, 0].astype(F32) + rs2[k, 1].astype(F32)
 
+    def experts(k):
+        fwd_right(k).wait_recv()
+        fwd_left(k).wait_recv()
+
+        rows = xall[k].reshape(4 * ROWS, width)
+        pre = dot(rows, wgu[...])
+        gate_cut = jnp.minimum(pre[:, :ff], clamp_limit)
+        up_cut = jnp.clip(pre[:, ff:], -clamp_limit, clamp_limit)
+        hidden = (
+            (up_cut + 1.0) * gate_cut * (1.0 / (1.0 + jnp.exp(-sigmoid_slope * gate_cut)))
+        ).astype(BF)
+        part[k] = dot(hidden, wd[...]).astype(BF).reshape(4, ROWS, width)
+        rs_far(k)
+
+    def pass_on(k):
+        rs_far_left(k).wait_recv()
+        part[k, 1, :, cols_a] = (
+            part[k, 1, :, cols_a].astype(F32) + rs1[k, 0].astype(F32)
+        ).astype(BF)
+        rs_near_left(k, cols_a, 2).start()
+        rs_far_right(k).wait_recv()
+        part[k, 2, :, cols_b] = (
+            part[k, 2, :, cols_b].astype(F32) + rs1[k, 1].astype(F32)
+        ).astype(BF)
+        rs_near_right(k, cols_b, 5).start()
+
+    def finish(k):
+        ret_out[k] = to_blocks(rs_total(k).astype(BF))
+        to_plane(k, give_back)
+
     def take_back(j):
         kk = mirror(j)
         wait_plane(kk, ret_in, r_recv)
@@ -501,51 +531,30 @@
             ag_left(k).wait_recv()
             fwd_left(k).start()
 
-        @pl.when((step >= 2) & (step < nz + 2))
-        def _():
-            k = step - 2
-            fwd_right(k).wait_recv()
-            fwd_left(k).wait_recv()
-
-            @pl.when(step == 2)
-            def _():
-                for copy in w_copies:
-                    copy.wait()
-
-            rows = xall[k].reshape(4 * ROWS, width)
-            pre = dot(rows, wgu[...])
-            gate_cut = jnp.minimum(pre[:, :ff], clamp_limit)
-            up_cut = jnp.clip(pre[:, ff:], -clamp_limit, clamp_limit)
-            hidden = (
-                (up_cut + 1.0) * gate_cut * (1.0 / (1.0 + jnp.exp(-sigmoid_slope * gate_cut)))
-            ).astype(BF)
-            part[k] = dot(hidden, wd[...]).astype(BF).reshape(4, ROWS, width)
-            rs_far(k)
-
-        def pass_on(k):
-            rs_far_left(k).wait_recv()
-            part[k, 1, :, cols_a] = (
-                part[k, 1, :, cols_a].astype(F32) + rs1[k, 0].astype(F32)
-            ).astype(BF)
-            rs_near_left(k, cols_a, 2).start()
-            rs_far_right(k).wait_recv()
-            part[k, 2, :, cols_b] = (
-                part[k, 2, :, cols_b].astype(F32) + rs1[k, 1].astype(F32)
-            ).astype(BF)
-            rs_near_right(k, cols_b, 5).start()
-
-        @pl.when((step >= 3) & (step < nz + 3))
+        @pl.when(step == 2)
+        def _():
+            for copy in w_copies:
+                copy.wait()
+
+        @pl.when((step >= 3) & (step < nz + 2))
+        def _():
+            experts(step - 2)
+
+        @pl.when((step >= 4) & (step < nz + 3))
         def _():
             pass_on(step - 3)
 
-        @pl.when((step >= 2) & (step < nz + 2))
+        @pl.when((step >= 3) & (step < nz + 2))
         def _():
             rs_near(step - 2)
 
+        @pl.when(step == nz + 1)
+        def _():
+            experts(0)
+
         @pl.when(step == nz + 2)
         def _():
-            rs_far(nz)
-            rs_near(nz)
+            rs_near(0)
 
         @pl.when((step >= 2) & (step <= nz // 2))
         def _():
@@ -608,33 +617,35 @@
 
             each_plane(step - 4, attend_to)
 
-        @pl.when(step >= 4)
-        def _():
-            k = step - 4
-            ret_out[k] = to_blocks(rs_total(k).astype(BF))
-
-            @pl.when(k == 0)
-            def _():
-                ret_in[0, p_me] = ret_out[0, p_me]
-
-            to_plane(k, give_back)
+        @pl.when(step >= 5)
+        def _():
+            finish(step - 4)
 
         @pl.when(step == nz)
         def _():
             part[nz] = project()
 
+        @pl.when(step == nz + 2)
+        def _():
+            pass_on(0)
+            rs_far(nz)
+            rs_near(nz)
+
         @pl.when(step == nz + 3)
         def _():
+            finish(jnp.int32(0))
+            ret_in[0, p_me] = ret_out[0, p_me]
             pass_on(nz)
 
-        @pl.when(step >= nz - 1)
+        @pl.when(step >= nz)
         def _():
             take_back(step - (nz - 1))
-
-    mix_ref[...] = rms_scale(rs_total(nz), mg_ref[...]).astype(BF)
 
     for j in (5, 6, 7):
         take_back(jnp.int32(j))
+
+    mix_ref[...] = rms_scale(rs_total(nz), mg_ref[...]).astype(BF)
+    take_back(jnp.int32(0))
 
     columns_of = side[...].T
     at0, at1, weight0, weight1 = (columns_of[:, c : c + 1] for c in range(4))
@@ -659,24 +670,6 @@
     wait_bytes(kv.at[pl.ds(0, nz - 1), 0, 0], kz_send.at[0])
     wait_bytes(kv.at[:, 0, pl.ds(0, 3)], ky_send.at[0])
     wait_bytes(kv.at[:, 0], kc_send.at[0])
-
-
-def hand_over(mix_hbm, rows_hbm, mix_out, rows_out, mix_v, rows_v, sems):
-    taken = [
-        pltpu.make_async_copy(mix_hbm, mix_v, sems.at[0]),
-        pltpu.make_async_copy(rows_hbm, rows_v, sems.at[1]),
-    ]
-    given = [
-        pltpu.make_async_copy(mix_v, mix_out, sems.at[2]),
-        pltpu.make_async_copy(rows_v, rows_out, sems.at[3]),
-    ]
-    for copy in taken:
-        copy.start()
-    for here, there in zip(taken, given):
-        here.wait()
-        there.start()
-    for copy in given:
-        copy.wait()
 
 
 def permutation():
@@ -740,8 +733,8 @@
     matrix = permutation()
     pin = jnp.asarray(matrix, BF)
     pout = jnp.asarray(matrix.T, BF)
+    hbm = pl.BlockSpec(memory_space=pltpu.HBM)
     vmem = pl.BlockSpec(memory_space=pltpu.VMEM)
-    hbm = pl.BlockSpec(memory_space=pl.ANY)
     travel = (nz, PL, ROWS, width // SUB)
     dma = pltpu.SemaphoreType.DMA
     operands = (
@@ -764,8 +757,8 @@
     made = pl.pallas_call(
         functools.partial(layer_kernel, nz),
         out_shape=(
-            jax.ShapeDtypeStruct((seq // TP, width), BF),
-            jax.ShapeDtypeStruct((tok, width), BF),
+            pltpu.VMEM((seq // TP, width), BF),
+            pltpu.VMEM((tok, width), BF),
         ),
         in_specs=[hbm] * (OPERANDS + 4),
         out_specs=(vmem, vmem),
@@ -811,7 +804,7 @@
             dma((OPERANDS,)),
         ],
         compiler_params=pltpu.CompilerParams(
-            collective_id=0, has_side_effects=True, vmem_limit_bytes=62 * 2**20
+            collective_id=0, has_side_effects=True, vmem_limit_bytes=58 * 2**20
         ),
         name="layer",
     )(
@@ -821,16 +814,7 @@
         down_w,
         out_weight,
     )
-    return tuple(
-        pl.pallas_call(
-            hand_over,
-            out_shape=tuple(jax.ShapeDtypeStruct(a.shape, a.dtype) for a in made),
-            in_specs=[hbm] * 2,
-            out_specs=(hbm, hbm),
-            scratch_shapes=[pltpu.VMEM(a.shape, a.dtype) for a in made] + [dma((4,))],
-            name="hand_over",
-        )(*made)
-    )
+    return made
 
 
 def solution(mesh):

time: 140 us -> 137 us (0.979)
  Pallas kernels: 138 us -> 134 us
  local copies, waits for them, and re-layouts: 0 us -> 1.47 us
    pallas_call x2 -> x1, Pallas kernels: 138 us -> 134 us  [local(): pl.pallas_call(functools.partial(layer_kernel, nz), out_shape=(pltpu.VMEM...]
    unnamed x0 -> x2, local copies, waits for them, and re-layouts: none -> 1.47 us
where the time goes in v5:
time: 137 us
  Pallas kernels  134 us (98%)
  local copies, waits for them, and re-layouts  1.47 us (1%)
    pallas_call x1, Pallas kernels, local(): pl.pallas_call(functools.partial(layer_kernel, nz), out_shape=(pltpu.VMEM...  134 us

profile of v5, /device:TPU:1, one launch (start us, length us, event | category | flops | bytes accessed | tf_op | source)
XLA Modules:
  0.0 136.6 jit_solution(2689210524757764680)
XLA Ops:
  0.6 134.5 %layer.1 = (bf16[48,2048]{1,0:T(8,128)(2,1)S(1)}, bf16[128,2048]{1,0:T(8,128)(2,1)S(1)}) custom-call(bf16[128,2048]{1,0:T(8,128)(2,1)} %refs_0_.1, s32[2,128]{1,0:T(2,128)} %bitcast.10, f32[2,128]{1,0:T(2,128)} %bitcast.11, f32[1,2048]{1,0:T(1,128)} %bitcast.7, f32[1,2048]{1,0:T(1,128)} %bitcast.8, bf16[384,384]{1,0:T(8,128)(2,1)} %constant.14.clone.refs_5_.refs_6_, ...), custom_call_target="tpu_custom_call" | custom-call | tf_op jit(solution)/shard_map/layer/pallas_call | solution.py:757
  135.1 0.7 copy.25
  135.8 0.8 copy.26

commit v6 on v5

--- a/solution.py
+++ b/solution.py
@@ -64,8 +64,8 @@
     for copy in copies:
         copy.start()
 
-    def operands_here():
-        for copy in copies:
+    def operands_here(first, end):
+        for copy in copies[first:end]:
             copy.wait()
 
     layer(nz, operands_here, *held, *refs[OPERANDS : OPERANDS + 6], *refs[2 * OPERANDS + 6 : -1])
@@ -113,6 +113,7 @@
     ow,
     kv,
     side,
+    both,
     q_s,
     m_s,
     l_s,
@@ -190,7 +191,7 @@
     for copy in w_copies:
         copy.start()
 
-    operands_here()
+    operands_here(0, 7)
     xf = x_ref[...].astype(F32)
     normed[...] = rms_scale(xf, eg_ref[...]).astype(BF)
 
@@ -379,6 +380,7 @@
         gather(MIRROR[c])
         to_plane(jnp.int32(MIRROR[c]), dispatch)
 
+    operands_here(7, OPERANDS)
     grid_rows = k_ref.shape[0] // GRID_W
     first_row = (z * PL + p_me) * grid_rows
     cosine = jnp.concatenate(
@@ -412,6 +414,7 @@
 
     for h in range(HEADS):
         q_s[h] = normed_and_turned(q_ref[:, h * HEAD : (h + 1) * HEAD], qg_ref[...])
+    ret_rows[0] = jnp.zeros(ret_rows.shape[1:], BF)
     m_s[...] = jnp.full(m_s.shape, -1e30, F32)
     l_s[...] = jnp.zeros(l_s.shape, F32)
     acc_s[...] = jnp.zeros(acc_s.shape, F32)
@@ -556,6 +559,14 @@
         def _():
             rs_near(0)
 
+        @pl.when((step >= 4) & (step <= nz // 2 + 4))
+        def _():
+            def attend_to(j):
+                kv_across(j).wait_recv()
+                attend(j)
+
+            each_plane(step - 4, attend_to)
+
         @pl.when((step >= 2) & (step <= nz // 2))
         def _():
             below, above = 2 * step - 3, 2 * step - 2
@@ -609,14 +620,6 @@
 
             each_plane(step - 3, across)
 
-        @pl.when((step >= 4) & (step <= nz // 2 + 4))
-        def _():
-            def attend_to(j):
-                kv_across(j).wait_recv()
-                attend(j)
-
-            each_plane(step - 4, attend_to)
-
         @pl.when(step >= 5)
         def _():
             finish(step - 4)
@@ -643,20 +646,23 @@
 
     for j in (5, 6, 7):
         take_back(jnp.int32(j))
-
-    mix_ref[...] = rms_scale(rs_total(nz), mg_ref[...]).astype(BF)
-    take_back(jnp.int32(0))
 
     columns_of = side[...].T
     at0, at1, weight0, weight1 = (columns_of[:, c : c + 1] for c in range(4))
     lanes = lax.broadcasted_iota(jnp.int32, (tok, nz * ROWS), 1).astype(F32)
     take = jnp.concatenate([one_hot(lanes == at0), one_hot(lanes == at1)], axis=0)
+    block = min(512, width)
+    blocks = [slice(c * block, (c + 1) * block) for c in range(width // block)]
+    for columns in blocks:
+        both[:, columns] = dot(take, ret_rows[:, :, columns].reshape(nz * ROWS, block))
+
+    mix_ref[...] = rms_scale(rs_total(nz), mg_ref[...]).astype(BF)
+
+    take_back(jnp.int32(0))
     square = jnp.zeros((tok, 1), F32)
-    block = min(512, width)
-    for c in range(width // block):
-        columns = slice(c * block, (c + 1) * block)
-        both = dot(take, ret_rows[:, :, columns].reshape(nz * ROWS, block))
-        mixed = weight0 * both[:tok] + weight1 * both[tok:]
+    for columns in blocks:
+        results = both[:, columns] + dot(take[:, :ROWS], ret_rows[0, :, columns])
+        mixed = weight0 * results[:tok] + weight1 * results[tok:]
         combined[:, columns] = mixed
         square = square + jnp.sum(mixed * mixed, axis=1, keepdims=True)
     scale = lax.rsqrt(square / width + norm_eps)
@@ -780,6 +786,7 @@
             pltpu.VMEM(out_weight.shape, BF),
             pltpu.VMEM((nz, 2, 4, 2, seq, HEAD), BF),
             pltpu.VMEM((8, tok), F32),
+            pltpu.VMEM((2 * tok, width), F32),
             pltpu.VMEM((HEADS, seq, HEAD), BF),
             pltpu.VMEM((HEADS, seq, HEAD), F32),
             pltpu.VMEM((HEADS, seq, HEAD), F32),

time: 137 us -> 137 us (level)
  no operation moved by 1% of the time
where the time goes in v6:
time: 137 us
  Pallas kernels  135 us (99%)
  local copies, waits for them, and re-layouts  1.47 us (1%)
    pallas_call x1, Pallas kernels, local(): pl.pallas_call(functools.partial(layer_kernel, nz), out_shape=(pltpu.VMEM...  135 us

profile of v6, /device:TPU:1, one launch (start us, length us, event | category | flops | bytes accessed | tf_op | source)
XLA Modules:
  0.0 136.8 jit_solution(7196573543251262043)
XLA Ops:
  0.6 134.7 %layer.1 = (bf16[48,2048]{1,0:T(8,128)(2,1)S(1)}, bf16[128,2048]{1,0:T(8,128)(2,1)S(1)}) custom-call(bf16[128,2048]{1,0:T(8,128)(2,1)} %refs_0_.1, s32[2,128]{1,0:T(2,128)} %bitcast.10, f32[2,128]{1,0:T(2,128)} %bitcast.11, f32[1,2048]{1,0:T(1,128)} %bitcast.7, f32[1,2048]{1,0:T(1,128)} %bitcast.8, bf16[384,384]{1,0:T(8,128)(2,1)} %constant.14.clone.refs_5_.refs_6_, ...), custom_call_target="tpu_custom_call" | custom-call | tf_op jit(solution)/shard_map/layer/pallas_call | solution.py:763
  135.3 0.7 copy.25
  136.0 0.8 copy.26

commit v7 on v6

--- a/solution.py
+++ b/solution.py
@@ -64,8 +64,8 @@
     for copy in copies:
         copy.start()
 
-    def operands_here(first, end):
-        for copy in copies[first:end]:
+    def operands_here():
+        for copy in copies:
             copy.wait()
 
     layer(nz, operands_here, *held, *refs[OPERANDS : OPERANDS + 6], *refs[2 * OPERANDS + 6 : -1])
@@ -191,7 +191,7 @@
     for copy in w_copies:
         copy.start()
 
-    operands_here(0, 7)
+    operands_here()
     xf = x_ref[...].astype(F32)
     normed[...] = rms_scale(xf, eg_ref[...]).astype(BF)
 
@@ -380,7 +380,6 @@
         gather(MIRROR[c])
         to_plane(jnp.int32(MIRROR[c]), dispatch)
 
-    operands_here(7, OPERANDS)
     grid_rows = k_ref.shape[0] // GRID_W
     first_row = (z * PL + p_me) * grid_rows
     cosine = jnp.concatenate(
@@ -559,14 +558,6 @@
         def _():
             rs_near(0)
 
-        @pl.when((step >= 4) & (step <= nz // 2 + 4))
-        def _():
-            def attend_to(j):
-                kv_across(j).wait_recv()
-                attend(j)
-
-            each_plane(step - 4, attend_to)
-
         @pl.when((step >= 2) & (step <= nz // 2))
         def _():
             below, above = 2 * step - 3, 2 * step - 2
@@ -619,6 +610,14 @@
                 kv_across(j).start()
 
             each_plane(step - 3, across)
+
+        @pl.when((step >= 4) & (step <= nz // 2 + 4))
+        def _():
+            def attend_to(j):
+                kv_across(j).wait_recv()
+                attend(j)
+
+            each_plane(step - 4, attend_to)
 
         @pl.when(step >= 5)
         def _():

time: 137 us -> 136 us (level)
  no operation moved by 1% of the time
where the time goes in v7:
time: 136 us
  Pallas kernels  134 us (99%)
  local copies, waits for them, and re-layouts  1.47 us (1%)
    pallas_call x1, Pallas kernels, local(): pl.pallas_call(functools.partial(layer_kernel, nz), out_shape=(pltpu.VMEM...  134 us

profile of v7, /device:TPU:1, one launch (start us, length us, event | category | flops | bytes accessed | tf_op | source)
XLA Modules:
  0.0 136.3 jit_solution(11160651027350009429)
XLA Ops:
  0.6 134.1 %layer.1 = (bf16[48,2048]{1,0:T(8,128)(2,1)S(1)}, bf16[128,2048]{1,0:T(8,128)(2,1)S(1)}) custom-call(bf16[128,2048]{1,0:T(8,128)(2,1)} %refs_0_.1, s32[2,128]{1,0:T(2,128)} %bitcast.10, f32[2,128]{1,0:T(2,128)} %bitcast.11, f32[1,2048]{1,0:T(1,128)} %bitcast.7, f32[1,2048]{1,0:T(1,128)} %bitcast.8, bf16[384,384]{1,0:T(8,128)(2,1)} %constant.14.clone.refs_5_.refs_6_, ...), custom_call_target="tpu_custom_call" | custom-call | tf_op jit(solution)/shard_map/layer/pallas_call | solution.py:762
  134.8 0.7 copy.25
  135.5 0.8 copy.26
